TPU v7x, 128 devices: a whole 4x4x4 slice. The times are simulated.
128 devices in a mesh: ep: 32 (over z, y, core), tp: 4 (over x).
Axes of the slice: x: 4, y: 4, z: 4, core: 2. Of those that a mesh axis runs over, the one named last changes fastest.
Arguments:
- query_rows: bfloat16 [32768, 1024], P('ep', 'tp'), may hold values from -140 to 140
- key_rows: bfloat16 [32768, 256], P('ep', 'tp'), may hold values from -4.5 to 4.5
- value_rows: bfloat16 [32768, 256], P('ep', 'tp'), may hold values from -6 to 6
- sink_logit: float32 [16], P('tp'), may hold values from 1 to 6
- out_weight: bfloat16 [1024, 2048], P('tp'), may hold values from -0.1875 to 0.1875
- routed_rows: bfloat16 [16384, 2048], P(('ep', 'tp')), may hold values from -6 to 6
- norm_gain: float32 [2048], replicated, may hold values from 0.1 to 1.9
- routing: int32 [16384, 2], P(('ep', 'tp')), may hold values from 0 to 31, all different within a row; in each aligned block of 128 rows (0 to 127, 128 to 255, ...) at most 9 rows name the same one
- route_weight: float32 [16384, 2], P(('ep', 'tp')), may hold values from 0.2 to 1
- gate_weight: bfloat16 [32, 2048, 7168], P('ep', None, 'tp'), may hold values from -0.125 to 0.125
- up_weight: bfloat16 [32, 2048, 7168], P('ep', None, 'tp'), may hold values from -0.125 to 0.125
- down_weight: bfloat16 [32, 7168, 2048], P('ep', 'tp'), may hold values from -0.0625 to 0.0625
Outputs:
- mixed_rows: bfloat16 [32768, 2048], P(('ep', 'tp'))
- expert_mix: bfloat16 [16384, 2048], P(('ep', 'tp'))
Inputs may be any that keep to these rules, and one draw needn't show every extreme that they name: `routing`: each token names 2 different experts. Within the 128 rows of one device no expert is named by more than 9 rows, and in every draw some device's rows name some expert exactly 9 times.
All inputs are finite; a program needn't handle non-finite values.
Results may differ from a plain program's by a relative error of at most 0.012.
Values may be sent and summed in bfloat16 or wider, within the bound.
No kernel may reach another device: no remote copies, remote signals or barrier semaphores. Data moves between devices by JAX's collectives and lax.ppermute only.
A program may use at most 128 MiB of HBM per device.

v0:
```python
import jax
import jax.numpy as jnp
from jax import lax
from jax.sharding import PartitionSpec as P

HEAD_DIM = 64
WINDOW = 128


EPS = 1e-06


def padded_2(value, sides, width):
    for axis, dim in sides:
        peers, length = (lax.axis_size(axis), value.shape[dim])
        up = [(i, (i + 1) % peers) for i in range(peers - 1)]
        down = [(j, i) for i, j in up]
        last = lax.slice_in_dim(value, length - width, length, axis=dim)
        leading = lax.slice_in_dim(value, 0, width, axis=dim)
        before = lax.ppermute(last, axis, up)
        after = lax.ppermute(leading, axis, down)
        value = jnp.concatenate([before, value, after], axis=dim)
    return value


def split_up(value, dim, peers):
    dims = value.shape
    pieces = value.reshape(*dims[:dim], peers, dims[dim] // peers, *dims[dim + 1 :])
    return jnp.moveaxis(pieces, dim, 0)


def sum_at_owner(value, axis, dim):
    peers = lax.axis_size(axis)
    pieces = lax.all_to_all(split_up(value, dim, peers), axis, 0, 0, tiled=True)
    return jnp.sum(pieces.astype(jnp.float32), axis=0)


def items_in_groups(value, axis, split_dim, concat_dim, work, item_dim, out_dim):
    items = jax.tree.leaves(value)[0].shape[item_dim]
    count = 4 if items % 4 == 0 else 1
    done = []
    for k in range(count):
        group = jax.tree.map(
            lambda a: lax.slice_in_dim(
                a, k * (items // count), (k + 1) * (items // count), axis=item_dim
            ),
            value,
        )
        done.append(
            work(
                lax.all_to_all(
                    group, axis, split_axis=split_dim, concat_axis=concat_dim, tiled=True
                )
            )
        )
    return jax.tree.map(lambda *parts: jnp.concatenate(parts, axis=out_dim), *done)


def expert_hidden(arrived, gate_weight, up_weight):
    gate_pre = jnp.einsum(
        "scd,df->scf", arrived, gate_weight[0], preferred_element_type=jnp.float32
    )
    up_pre = jnp.einsum("scd,df->scf", arrived, up_weight[0], preferred_element_type=jnp.float32)
    return (jax.nn.silu(gate_pre) * up_pre).astype(jnp.bfloat16)


def window_attention(query_rows, key_rows, value_rows, sink_logit):
    row_count = query_rows.shape[0]
    kv_here = key_rows.shape[1] // HEAD_DIM
    group_size = query_rows.shape[1] // (kv_here * HEAD_DIM)
    block_rows = min(512, row_count)
    joined = jnp.concatenate([key_rows, value_rows], axis=1)
    padded = padded_2(joined, (("ep", 0),), WINDOW)
    seq_total = row_count * lax.axis_size("ep")
    offset = lax.axis_index("ep") * row_count
    sink_col = sink_logit.reshape(kv_here, group_size)[:, :, None]
    score_scale = HEAD_DIM ** (-0.5)

    def one_block(block_index):
        first_row = block_index * block_rows
        query_block = lax.dynamic_slice_in_dim(query_rows, first_row, block_rows, 0).reshape(
            block_rows, kv_here, group_size, HEAD_DIM
        )
        key_span = lax.dynamic_slice_in_dim(padded, first_row, block_rows + 2 * WINDOW, 0)
        key_block = key_span[:, : kv_here * HEAD_DIM].reshape(-1, kv_here, HEAD_DIM)
        value_block = key_span[:, kv_here * HEAD_DIM :].reshape(-1, kv_here, HEAD_DIM)
        scores = (
            jnp.einsum("qkgd,skd->kgqs", query_block, key_block, preferred_element_type=jnp.float32)
            * score_scale
        )
        query_pos = first_row + jnp.arange(block_rows, dtype=jnp.int32)
        key_pos = first_row - WINDOW + jnp.arange(block_rows + 2 * WINDOW, dtype=jnp.int32)
        global_pos = offset + key_pos
        inside = (
            (jnp.abs(key_pos[None, :] - query_pos[:, None]) <= WINDOW)
            & (global_pos >= 0)[None, :]
            & (global_pos < seq_total)[None, :]
        )
        scores = jnp.where(inside, scores, -jnp.inf)
        row_peak = jnp.maximum(jnp.max(scores, axis=-1), sink_col)
        weights = jnp.exp(scores - row_peak[..., None])
        total_weight = jnp.sum(weights, axis=-1) + jnp.exp(sink_col - row_peak)
        attended = jnp.einsum(
            "kgqs,skd->qkgd",
            weights.astype(jnp.bfloat16),
            value_block,
            preferred_element_type=jnp.float32,
        )
        attended = attended / jnp.transpose(total_weight, (2, 0, 1))[..., None]
        return attended.reshape(block_rows, -1).astype(jnp.bfloat16)

    pieces = lax.map(one_block, jnp.arange(row_count // block_rows, dtype=jnp.int32))
    return pieces.reshape(row_count, -1)


def body(
    query_rows,
    key_rows,
    value_rows,
    sink_logit,
    out_weight,
    routed_rows,
    norm_gain,
    routing,
    route_weight,
    gate_weight,
    up_weight,
    down_weight,
):
    attended = window_attention(query_rows, key_rows, value_rows, sink_logit)
    projected = lax.psum_scatter(
        jnp.dot(attended, out_weight, preferred_element_type=jnp.float32).astype(jnp.bfloat16),
        "tp",
        scatter_dimension=0,
        tiled=True,
    )
    token_count, model_width = routed_rows.shape
    top_count = routing.shape[1]
    experts = lax.axis_size("ep")
    capacity = token_count * top_count * 9 // (8 * experts)
    values = routed_rows.astype(jnp.float32)
    normed = (
        values * lax.rsqrt(jnp.mean(values * values, axis=-1, keepdims=True) + EPS) * norm_gain
    ).astype(jnp.bfloat16)
    chosen = routing.reshape(-1)
    onehot = (chosen[:, None] == jnp.arange(experts, dtype=jnp.int32)[None, :]).astype(jnp.int32)
    before = jnp.cumsum(onehot, axis=0) - onehot
    slot_index = jnp.sum(before * onehot, axis=1)
    target = chosen * capacity + slot_index
    outgoing = (
        jnp.zeros((experts * capacity, model_width), jnp.bfloat16)
        .at[target]
        .set(jnp.repeat(normed, top_count, axis=0))
    )
    outgoing = outgoing.reshape(experts, capacity, model_width)

    def expert_sectioned(arrived):
        hidden = expert_hidden(
            lax.all_gather(arrived, "tp", axis=0, tiled=True), gate_weight, up_weight
        )
        rounded = jnp.einsum(
            "scf,fd->scd", hidden, down_weight[0], preferred_element_type=jnp.float32
        ).astype(jnp.bfloat16)
        summed = sum_at_owner(
            lax.optimization_barrier(rounded).astype(jnp.float32).astype(jnp.bfloat16), "tp", 0
        )
        return lax.all_to_all(
            summed.astype(jnp.bfloat16), "ep", split_axis=0, concat_axis=0, tiled=True
        ).astype(summed.dtype)

    results = items_in_groups(outgoing, "ep", 0, 0, expert_sectioned, 1, 1)
    slot_results = results.reshape(experts * capacity, model_width)
    picked = slot_results[target] * route_weight.reshape(-1)[:, None]
    expert_mix = jnp.sum(picked.reshape(token_count, top_count, model_width), axis=1).astype(
        jnp.bfloat16
    )
    return (projected, expert_mix)


def solution(mesh):
    in_specs = (
        P("ep", "tp"),
        P("ep", "tp"),
        P("ep", "tp"),
        P("tp"),
        P("tp", None),
        P(("ep", "tp"), None),
        P(),
        P(("ep", "tp"), None),
        P(("ep", "tp"), None),
        P("ep", None, "tp"),
        P("ep", None, "tp"),
        P("ep", "tp", None),
    )
    out_specs = (P(("ep", "tp"), None), P(("ep", "tp"), None))
    return jax.shard_map(body, mesh=mesh, in_specs=in_specs, out_specs=out_specs, check_vma=False)
```

profile of v0, /device:TPU:0, one launch (start us, length us, event | category | flops | bytes accessed | tf_op | source)
XLA Modules:
  0.0 272.0 jit_solution(11826062474658149984)
XLA Ops:
  13.8 3.2 %scatter_custom_fusion = bf16[288,2048]{1,0:T(8,128)(2,1)} fusion(s32[256]{0:T(256)S(1)} %bitcast.150, bf16[256,2048]{1,0:T(8,128)(2,1)S(1)} %reshape.297, bf16[]{:T(256)} %constant.86.clone.1), kind=kCustom, calls=%fused_computation.50 | custom fusion | bytes 1179650 | tf_op jit(solution)/shard_map/scatter | solution.py:153
  18.6 36.7 %all_to_all.15 = bf16[32,9,2048]{2,1,0:T(8,128)(2,1)S(1)} all-to-all(bf16[32,9,2048]{2,1,0:T(8,128)(2,1)S(1)} %reshape.279), channel_id=1, replica_groups=mesh['ep'=32,'tp'=4] {'ep'}, dimensions={0} | all-to-all | bytes 2359296 | tf_op jit(solution)/shard_map/all_to_all | solution.py:51
  55.3 1.8 copy.45
  57.2 2.0 collective-permute-start
  60.8 1.7 collective-permute-done.1
  62.5 26.7 %while.12 = (s32[]{:T(128)}, bf16[2,512,256]{2,1,0:T(8,128)(2,1)S(1)}, s32[2]{0:T(128)S(1)}, bf16[1280,128]{0,1:T(8,128)(2,1)S(1)}, s32[]{:T(128)}, /*index=5*/b...) while((s32[]{:T(128)}, ...), condition=%wide.region_3.4_spmd, body=%wide.region_0.3_spmd.sunk | while | flops 422191360 | bytes 48526672 | solution.py:112
  67.1 2.6 copy-done.2
  71.2 4.5 %fusion.71 = bf16[512,1,4,64]{0,3,2,1:T(8,128)(2,1)S(1)} fusion(f32[768,512,4]{1,0,2:T(8,128)} %copy-done.2, f32[4,512]{1,0:T(4,128)S(1)} %broadcast_maximum_fusion.2, pred[512,768]{0,1:T(8,128)(4,1)S(1)} %fusion.67, f32[512,4]{0,1:T(4,128)S(1)} %fusion.70, bf16[1280,128]{0,1:T(8,128)(2,1)S(1)} %get-tuple-element.222, s32[]{:T(128)S(6)} %select_n.57, ...), kind=kOutput, calls=%fused_computation.15.clone.1 | convolution fusion | flops 207880192 | bytes 7061512 | tf_op jit(solution)/shard_map/while/body/eval_jaxpr/kgqs,skd->qkgd/dot_general | solution.py:103
  80.5 2.6 copy-done.2
  84.5 4.6 %fusion.71 = bf16[512,1,4,64]{0,3,2,1:T(8,128)(2,1)S(1)} fusion(f32[768,512,4]{1,0,2:T(8,128)} %copy-done.2, f32[4,512]{1,0:T(4,128)S(1)} %broadcast_maximum_fusion.2, pred[512,768]{0,1:T(8,128)(4,1)S(1)} %fusion.67, f32[512,4]{0,1:T(4,128)S(1)} %fusion.70, bf16[1280,128]{0,1:T(8,128)(2,1)S(1)} %get-tuple-element.222, s32[]{:T(128)S(6)} %select_n.57, ...), kind=kOutput, calls=%fused_computation.15.clone.1 | convolution fusion | flops 207880192 | bytes 7061512 | tf_op jit(solution)/shard_map/while/body/eval_jaxpr/kgqs,skd->qkgd/dot_general | solution.py:103
  89.3 3.2 %convolution_convert_fusion = bf16[1024,2048]{1,0:T(8,128)(2,1)} fusion(bf16[1024,256]{1,0:T(8,128)(2,1)S(1)} %bitcast.146, bf16[256,2048]{1,0:T(8,128)(2,1)S(1)} %copy-done), kind=kOutput, calls=%fused_computation.43 | convolution fusion | flops 1075838976 | bytes 5767168 | tf_op jit(solution)/shard_map/dot_general | solution.py:132
  92.5 15.0 %all-gather.2.cloned.1.call-done = bf16[128,9,2048]{2,0,1:T(8,128)(2,1)} async-done(((bf16[32,9,2048]{2,0,1:T(8,128)(2,1)}), bf16[128,9,2048]{2,0,1:T(8,128)(2,1)}) %all-gather.2.cloned.1.call-update) | async-done | bytes 4718608 | tf_op jit(solution)/shard_map/all_gather | solution.py:159
  107.5 14.7 %fusion.28 = f32[128,9,1792]{2,0,1:T(8,128)} fusion(bf16[128,9,2048]{2,0,1:T(8,128)(2,1)} %all-gather.2.cloned.1.call-done, bf16[1,2048,1792]{2,1,0:T(8,128)(2,1)} %param.24), kind=kOutput, calls=%fused_computation.37 | convolution fusion | flops 8455716864 | bytes 20316160 | tf_op jit(solution)/shard_map/scd,df->scf/dot_general | solution.py:63
  122.2 28.4 %fusion.37 = bf16[128,9,2048]{2,0,1:T(8,128)(2,1)} fusion(bf16[1,1792,2048]{2,1,0:T(8,128)(2,1)} %param.25, f32[128,9,1792]{2,0,1:T(8,128)} %fusion.28, bf16[128,9,2048]{2,0,1:T(8,128)(2,1)} %all-gather.2.cloned.1.call-done, bf16[1,2048,1792]{2,1,0:T(8,128)(2,1)} %param.23), kind=kOutput, calls=%fused_computation.42 | convolution fusion | flops 16926179328 | bytes 32374784 | tf_op jit(solution)/shard_map/scf,fd->scd/dot_general | solution.py:161
  150.6 2.8 %copy.46 = bf16[4,32,9,2048]{3,1,2,0:T(8,128)(2,1)S(1)} copy(bf16[4,32,9,2048]{3,1,0,2:T(8,128)(2,1)} %bitcast.145) | data formatting | bytes 9437184 | tf_op jit(solution)/shard_map/reshape | solution.py:28
  153.4 58.0 %all_to_all.16 = bf16[4,32,9,2048]{3,1,2,0:T(8,128)(2,1)} all-to-all(bf16[4,32,9,2048]{3,1,2,0:T(8,128)(2,1)S(1)} %copy.46), channel_id=1, replica_groups=mesh['ep'=32,'tp'=4] {'tp'}, dimensions={0} | all-to-all | bytes 9437184 | tf_op jit(solution)/shard_map/all_to_all | solution.py:34
  211.4 3.3 %reduce_sum.55 = bf16[32,9,2048]{2,0,1:T(8,128)(2,1)S(1)} reduce(bf16[4,32,9,2048]{3,1,2,0:T(8,128)(2,1)} %all_to_all.16, bf16[]{:T(256)} %constant.86.clone.1), dimensions={0}, to_apply=%region_10.11 | reduce | flops 1769472 | bytes 5898242 | tf_op jit(solution)/shard_map/reduce_sum | solution.py:35
  214.8 2.0 copy.48
  216.8 7.7 %all-to-all-start.2 = ((bf16[32,9,2048]{2,1,0:T(8,128)(2,1)}), bf16[32,9,2048]{2,1,0:T(8,128)(2,1)}, u32[]{:S(2)}, u32[]{:S(2)}) async-start(bf16[32,9,2048]{2,1,0:T(8,128)(2,1)} %copy.48), calls=%async_computation.3 | async-start | bytes 4194304 | tf_op jit(solution)/shard_map/all_to_all | solution.py:167
  224.6 29.6 %all-to-all-done.2 = bf16[32,9,2048]{2,1,0:T(8,128)(2,1)} async-done(((bf16[32,9,2048]{2,1,0:T(8,128)(2,1)}), bf16[32,9,2048]{2,1,0:T(8,128)(2,1)}, u32[]{:S(2)}, u32[]{:S(2)}) %all-to-all-start.2) | async-done | bytes 1179680 | tf_op jit(solution)/shard_map/all_to_all | solution.py:167
  254.3 1.8 reshape.284
  256.1 2.7 gather_fusion
  258.8 2.5 gather.6
  261.3 3.9 %multiply_reduce_fusion = bf16[128,2048]{1,0:T(8,128)(2,1)} fusion(f32[128,2,2048]{2,1,0:T(2,128)S(1)} %gather.6, f32[128,2]{1,0:T(8,128)S(1)} %copy.49), kind=kLoop, calls=%fused_computation.44 | loop fusion | flops 786432 | bytes 2622464 | tf_op jit(solution)/shard_map/reduce_sum | solution.py:174
  (74 shorter events, 20.9 us)
Async XLA Ops:
  7.2 82.1 %copy-start = (bf16[256,2048]{1,0:T(8,128)(2,1)S(1)}, bf16[256,2048]{1,0:T(8,128)(2,1)}, u32[]{:S(2)}) copy-start(bf16[256,2048]{1,0:T(8,128)(2,1)} %param.18) | copy-start | bytes 3145732
  7.2 100.3 %all-gather.2.cloned.1.call-start = ((), (), s32[]{:S(2)}) async-start(), calls=%async_computation.5 | async-start | bytes 5898240 | tf_op jit(solution)/shard_map/all_gather | solution.py:159
  13.8 43.3 %copy-start.3 = (bf16[1024,64]{0,1:T(8,128)(2,1)S(1)}, bf16[1024,64]{0,1:T(8,128)(2,1)}, u32[]{:S(2)}) copy-start(bf16[1024,64]{0,1:T(8,128)(2,1)} %param.15) | copy-start | bytes 393220
  17.0 40.2 %copy-start.4 = (bf16[1024,64]{0,1:T(8,128)(2,1)S(1)}, bf16[1024,64]{0,1:T(8,128)(2,1)}, u32[]{:S(2)}) copy-start(bf16[1024,64]{0,1:T(8,128)(2,1)} %param.16) | copy-start | bytes 393220
  17.0 45.5 %copy-start.5 = (f32[4]{0:T(128)S(1)}, f32[4]{0:T(128)}, u32[]{:S(2)}) copy-start(f32[4]{0:T(128)} %param.17) | copy-start | bytes 52
  57.1 208.1 %reduce-scatter.2.cloned.1.call-start = ((), (), s32[]{:S(2)}) async-start(), calls=%async_computation.4 | async-start | bytes 5242880 | tf_op jit(solution)/shard_map/reduce_scatter | solution.py:131
  57.2 3.5 %collective-permute-start = (bf16[128,128]{0,1:T(8,128)(2,1)S(1)}, bf16[128,128]{0,1:T(8,128)(2,1)S(1)}, u32[]{:S(2)}, u32[]{:S(2)}) collective-permute-start(bf16[128,128]{0,1:T(8,128)(2,1)S(1)} %get-tuple-element.138), channel_id=1, source_target_pairs={{0,4},{4,8},{8,12},{12,16},{16,20},{20,24},{24,28},{28,32},{32,36}... | collective-permute-start | bytes 98312 | tf_op jit(solution)/shard_map/ppermute | solution.py:20
  59.3 3.2 %collective-permute-start.1 = (bf16[128,128]{0,1:T(8,128)(2,1)S(1)}, bf16[128,128]{0,1:T(8,128)(2,1)S(1)}, u32[]{:S(2)}, u32[]{:S(2)}) collective-permute-start(bf16[128,128]{0,1:T(8,128)(2,1)S(1)} %get-tuple-element.139), channel_id=1, source_target_pairs={{4,0},{8,4},{12,8},{16,12},{20,16},{24,20},{28,24},{32,28},{36,32}... | collective-permute-start | bytes 98312 | tf_op jit(solution)/shard_map/ppermute | solution.py:21
  67.1 2.7 copy-start.2
  80.4 2.7 copy-start.2
  211.4 13.1 %copy-start.6 = (f32[128,2]{0,1:T(2,128)S(1)}, f32[128,2]{0,1:T(2,128)}, u32[]{:S(2)}) copy-start(f32[128,2]{0,1:T(2,128)} %param.22) | copy-start | bytes 3076
  216.8 37.4 %all-to-all-start.2 = ((bf16[32,9,2048]{2,1,0:T(8,128)(2,1)}), bf16[32,9,2048]{2,1,0:T(8,128)(2,1)}, u32[]{:S(2)}, u32[]{:S(2)}) async-start(bf16[32,9,2048]{2,1,0:T(8,128)(2,1)} %copy.48), calls=%async_computation.3 | async-start | bytes 4194304 | tf_op jit(solution)/shard_map/all_to_all | solution.py:167
  256.0 9.2 %copy-start.1 = (bf16[256,2048]{1,0:T(8,128)(2,1)S(1)}, bf16[256,2048]{1,0:T(8,128)(2,1)}, u32[]{:S(2)}) copy-start(bf16[256,2048]{1,0:T(8,128)(2,1)} %param.18) | copy-start | bytes 3145732
Sparse Core Ops, SparseCore 0:
  57.2 50.2 all-gather.1
  110.5 47.2 reduce-scatter.1
where the time goes:
time: 273 us; the launch traced here: 272 us
  blocking collectives  94.7 us (35%)
  matrix products  57.8 us (21%)
  waiting for transfers between devices  46.4 us (17%)
  local copies, waits for them, and re-layouts  30.2 us (11%)
  other arithmetic  15.8 us (6%)
  between operations  14.3 us (5%)
  starting transfers between devices  11.2 us (4%)
    all_to_all x1, blocking collectives, sum_at_owner(): pieces = lax.all_to_all(split_up(value, dim, peers), axis, 0, 0, tiled=True)  58 us
    all_to_all x1, blocking collectives, items_in_groups(): lax.all_to_all(group, axis, split_axis=split_dim, concat_axis=concat_dim,...  36.7 us
    all_to_all x1, waiting for transfers between devices, expert_sectioned(): lax.all_to_all(summed.astype(jnp.bfloat16), 'ep', split_axis=0, concat_ax...  29.6 us
    dot_general x1, matrix products, expert_sectioned(): jnp.einsum('scf,fd->scd', hidden, down_weight[0], preferred_element_type=...  28.4 us
    all_gather x1, waiting for transfers between devices, expert_sectioned(): lax.all_gather(arrived, 'tp', axis=0, tiled=True)  15 us
    dot_general x1, matrix products, expert_hidden(): jnp.einsum('scd,df->scf', arrived, up_weight[0], preferred_element_type=j...  14.7 us
    dot_general x2, matrix products, one_block(): jnp.einsum('kgqs,skd->qkgd', weights.astype(jnp.bfloat16), value_block, p...  9.07 us
    all_to_all x1, starting transfers between devices, expert_sectioned(): lax.all_to_all(summed.astype(jnp.bfloat16), 'ep', split_axis=0, concat_ax...  7.66 us
  transfers between devices with their start and end apart: 5, of which 3 were waited for; matrix products, arithmetic and copies ran while one was open for 31% of the time, Pallas kernels for 0%

commit v1 on v0

v1 whole, which is shorter than its diff:
```python
import functools

import jax
import jax.numpy as jnp
from jax import lax
from jax.experimental import pallas as pl
from jax.experimental.pallas import tpu as pltpu
from jax.sharding import PartitionSpec as P


HEAD_DIM = 64
WINDOW = 128
EPS = 1e-06
CAP = 9
MAIN = 8
F32 = jnp.float32
BF16 = jnp.bfloat16


def dot(a, b, dims=((1,), (0,))):
    return lax.dot_general(a, b, (dims, ((), ())), preferred_element_type=F32)


def slot_iota(shape, experts):
    slot = lax.broadcasted_iota(jnp.int32, shape, 0)
    main = slot < experts * MAIN
    expert_of = jnp.where(main, lax.shift_right_logical(slot, 3), slot - experts * MAIN)
    return expert_of, jnp.where(main, slot & (MAIN - 1), MAIN)


def dispatch_kernel(rows_ref, gain_ref, routing_ref, weight_ref, out_ref, high_ref, low_ref, *, experts):
    tokens, width = rows_ref.shape
    x = rows_ref[...].astype(F32)
    mean = jnp.mean(x * x, axis=-1, keepdims=True)
    normed = (x * lax.rsqrt(mean + EPS) * gain_ref[...]).astype(BF16)
    ids = lax.broadcasted_iota(jnp.int32, (experts, tokens), 0)
    hot0 = routing_ref[0:1, :] == ids
    hot1 = routing_ref[1:2, :] == ids
    member = jnp.where(hot0 | hot1, 1.0, 0.0)
    row = lax.broadcasted_iota(jnp.int32, (tokens, tokens), 0)
    col = lax.broadcasted_iota(jnp.int32, (tokens, tokens), 1)
    upper = jnp.where(row <= col, 1.0, 0.0).astype(BF16)
    place = (dot(member.astype(BF16), upper) * member).astype(BF16)
    gate = jnp.where(hot0, weight_ref[0:1, :], 0.0) + jnp.where(hot1, weight_ref[1:2, :], 0.0)
    high = gate.astype(BF16)
    low = (gate - high.astype(F32)).astype(BF16)
    slots = experts * CAP
    expert_of, _ = slot_iota((slots, experts), experts)
    pick = jnp.where(expert_of == lax.broadcasted_iota(jnp.int32, (slots, experts), 1), 1.0, 0.0)
    pick = pick.astype(BF16)
    _, place_of = slot_iota((slots, tokens), experts)
    here = dot(pick, place) == (place_of + 1).astype(F32)
    high_ref[...] = jnp.where(here, dot(pick, high), 0.0).astype(BF16)
    low_ref[...] = jnp.where(here, dot(pick, low), 0.0).astype(BF16)
    rows = dot(jnp.where(here, 1.0, 0.0).astype(BF16), normed)
    last = []
    for j in range(width // 128):
        part = rows[:, j * 128 : (j + 1) * 128]
        tile = part[: experts * MAIN].reshape(experts, MAIN, 128).astype(BF16)
        out_ref[:, j * MAIN : (j + 1) * MAIN, :] = tile
        last.append(part[experts * MAIN :])
    out_ref[:, width // 128 * MAIN :, :] = jnp.stack(last, axis=1).astype(BF16)


def dispatch(routed_rows, norm_gain, routing, route_weight, experts):
    tokens, width = routed_rows.shape
    slots = experts * CAP
    matrix = jax.ShapeDtypeStruct((slots, tokens), BF16)
    return pl.pallas_call(
        functools.partial(dispatch_kernel, experts=experts),
        out_shape=(jax.ShapeDtypeStruct((experts, CAP * width // 128, 128), BF16), matrix, matrix),
        name="dispatch",
        cost_estimate=pl.CostEstimate(flops=400_000_000, transcendentals=0, bytes_accessed=2_500_000),
    )(routed_rows, norm_gain.reshape(1, width), routing.T, route_weight.T)


def attention_kernel(edge_ref, sink_ref, query_ref, kv_ref, vk_ref, out_ref):
    block = pl.program_id(0)
    size = WINDOW
    start = pl.multiple_of(block * size, size)
    kv = kv_ref[pl.ds(start, 3 * size), :]
    vk = vk_ref[pl.ds(start, 3 * size), :]
    lane = lax.broadcasted_iota(jnp.int32, (3 * size, 2 * HEAD_DIM), 1)
    left = lane < HEAD_DIM
    zero = jnp.zeros_like(kv)
    keys = jnp.concatenate([jnp.where(left, kv, zero), jnp.where(left, zero, vk)], axis=0)
    one = jnp.ones_like(kv)
    values = jnp.concatenate(
        [
            jnp.concatenate([jnp.where(left, vk, zero), jnp.where(left, one, zero)], axis=1),
            jnp.concatenate([jnp.where(left, zero, kv), jnp.where(left, zero, one)], axis=1),
        ],
        axis=0,
    )
    row = lax.broadcasted_iota(jnp.int32, (size, size), 0)
    col = lax.broadcasted_iota(jnp.int32, (size, size), 1)
    off_left = jnp.where((block == 0) & (edge_ref[0] == 1), 4 * size, 0)
    last = pl.num_programs(0) - 1
    off_right = jnp.where((block == last) & (edge_ref[1] == 1), 4 * size, 0)
    keep_left = col >= row + off_left
    keep_right = col + off_right <= row
    for pair in range(query_ref.shape[1] // (2 * HEAD_DIM)):
        lanes = slice(pair * 2 * HEAD_DIM, (pair + 1) * 2 * HEAD_DIM)
        query = query_ref[:, lanes] * jnp.asarray(HEAD_DIM**-0.5, BF16)
        scores = dot(query, keys, ((1,), (1,)))
        weights, sinks = [], []
        for one_head in range(2):
            low = one_head * 3 * size
            s0 = jnp.where(keep_left, scores[:, low : low + size], -jnp.inf)
            s1 = scores[:, low + size : low + 2 * size]
            s2 = jnp.where(keep_right, scores[:, low + 2 * size : low + 3 * size], -jnp.inf)
            sink = sink_ref[2 * pair + one_head]
            peak = jnp.max(jnp.maximum(jnp.maximum(s0, s1), s2), axis=1, keepdims=True)
            peak = jnp.maximum(peak, sink)
            weights += [jnp.exp(s - peak).astype(BF16) for s in (s0, s1, s2)]
            sinks.append(jnp.exp(sink - peak))
        total = dot(jnp.concatenate(weights, axis=1), values)
        lane_q = lax.broadcasted_iota(jnp.int32, (size, 2 * HEAD_DIM), 1)
        denominator = total[:, 2 * HEAD_DIM :] + jnp.where(lane_q < HEAD_DIM, sinks[0], sinks[1])
        out_ref[:, lanes] = (total[:, : 2 * HEAD_DIM] / denominator).astype(BF16)


def attention(query_rows, key_rows, value_rows, sink_logit):
    peers = lax.axis_size("ep")
    me = lax.axis_index("ep")
    up = [(i, i + 1) for i in range(peers - 1)]
    down = [(j, i) for i, j in up]
    joined = jnp.concatenate([key_rows, value_rows], axis=1)
    rows = joined.shape[0]
    before = lax.ppermute(joined[rows - WINDOW :], "ep", up)
    after = lax.ppermute(joined[:WINDOW], "ep", down)
    kv = jnp.concatenate([before, joined, after], axis=0)
    vk = jnp.concatenate([kv[:, HEAD_DIM:], kv[:, :HEAD_DIM]], axis=1)
    edge = jnp.stack([me == 0, me == peers - 1]).astype(jnp.int32)
    width = query_rows.shape[1]
    whole = lambda i: (0, 0)
    return pl.pallas_call(
        attention_kernel,
        grid=(rows // WINDOW,),
        in_specs=[
            pl.BlockSpec(memory_space=pltpu.SMEM),
            pl.BlockSpec(memory_space=pltpu.SMEM),
            pl.BlockSpec((WINDOW, width), lambda i: (i, 0)),
            pl.BlockSpec(kv.shape, whole),
            pl.BlockSpec(vk.shape, whole),
        ],
        out_specs=pl.BlockSpec((WINDOW, width), lambda i: (i, 0)),
        out_shape=jax.ShapeDtypeStruct((rows, width), BF16),
        name="attention",
        cost_estimate=pl.CostEstimate(flops=4_000_000_000, transcendentals=1_600_000, bytes_accessed=2_000_000),
    )(edge, sink_logit, query_rows, kv, vk)


def ring(shift):
    peers = lax.axis_size("tp")
    return [(i, (i + shift) % peers) for i in range(peers)]


def shift_tp(value, shift):
    return lax.ppermute(value, "tp", ring(shift))


def project_kernel(*refs):
    pieces = (len(refs) - 1) // 2
    out_ref = refs[-1]
    total = dot(refs[0][...], refs[pieces][...])
    for n in range(1, pieces):
        total += dot(refs[n][...], refs[pieces + n][...])
    out_ref[...] = total.astype(BF16)


def project(lefts, rights):
    rows = lefts[0].shape[0]
    width = rights[0].shape[1]
    step = 512
    return pl.pallas_call(
        project_kernel,
        grid=(width // step,),
        in_specs=[pl.BlockSpec(a.shape, lambda i: (0, 0)) for a in lefts]
        + [pl.BlockSpec((b.shape[0], step), lambda i: (0, i)) for b in rights],
        out_specs=pl.BlockSpec((rows, step), lambda i: (0, i)),
        out_shape=jax.ShapeDtypeStruct((rows, width), BF16),
        name="project",
        cost_estimate=pl.CostEstimate(flops=1_100_000_000, transcendentals=0, bytes_accessed=6_000_000),
    )(*lefts, *rights)


def fetch_weight(out_weight):
    peers = lax.axis_size("ep")
    half = out_weight.shape[0] // 2
    core = lax.axis_index("ep") % 2
    mine = lax.dynamic_slice_in_dim(out_weight, core * half, half, 0)
    swap = [(i, i ^ 1) for i in range(peers)]
    fetched = []
    for shift in (1, 3, 2):
        a = shift_tp(mine, shift)
        fetched.append((a, lax.ppermute(a, "ep", swap)))
    return fetched


def mix_tokens(attended, out_weight, fetched):
    peers = lax.axis_size("tp")
    me = lax.axis_index("tp")
    core = lax.axis_index("ep") % 2
    tokens = attended.shape[0] // peers
    half = out_weight.shape[0] // 2

    def block(shift):
        return lax.dynamic_slice_in_dim(attended, (me + shift) % peers * tokens, tokens, 0)

    lefts, rights = [block(0)], [out_weight]
    for shift, (a, b) in zip((1, 3, 2), fetched):
        heads = shift_tp(block(shift), shift)
        lefts.append(lax.dynamic_slice_in_dim(heads, core * half, half, 1))
        lefts.append(lax.dynamic_slice_in_dim(heads, (1 - core) * half, half, 1))
        rights += [a, b]
    return project(lefts, rights)


def expert_kernel(*refs, pieces):
    rows = refs[:pieces]
    gate_ref, up_ref, down_ref = refs[pieces : pieces + 3]
    outs = refs[pieces + 3 : 2 * pieces + 3]
    joined, total = refs[2 * pieces + 3 :]
    step = pl.program_id(0)
    count = rows[0].shape[0]

    @pl.when(step == 0)
    def _():
        for n in range(pieces):
            joined[n * count : (n + 1) * count, :] = rows[n][...]

    x = joined[...]
    gate = dot(x, gate_ref[...])
    up = dot(x, up_ref[...])
    hidden = (gate / (1.0 + jnp.exp(-gate)) * up).astype(BF16)
    part = dot(hidden, down_ref[...])

    @pl.when(step == 0)
    def _():
        total[...] = part

    @pl.when(step > 0)
    def _():
        total[...] += part

    @pl.when(step == pl.num_programs(0) - 1)
    def _():
        for n in range(pieces):
            outs[n][...] = total[n * count : (n + 1) * count, :].astype(BF16)


def expert(rows, gate_weight, up_weight, down_weight):
    pieces = len(rows)
    count, width = rows[0].shape
    units = gate_weight.shape[1]
    step = 256
    whole = pl.BlockSpec((count, width), lambda i: (0, 0))
    columns = pl.BlockSpec((width, step), lambda i: (0, i))
    return pl.pallas_call(
        functools.partial(expert_kernel, pieces=pieces),
        grid=(units // step,),
        in_specs=[whole] * pieces + [columns, columns, pl.BlockSpec((step, width), lambda i: (i, 0))],
        out_specs=[whole] * pieces,
        out_shape=[jax.ShapeDtypeStruct((count, width), BF16)] * pieces,
        scratch_shapes=[
            pltpu.VMEM((pieces * count, width), BF16),
            pltpu.VMEM((pieces * count, width), F32),
        ],
        name="expert",
        cost_estimate=pl.CostEstimate(
            flops=6 * pieces * count * width * units,
            transcendentals=pieces * count * units,
            bytes_accessed=6 * width * units,
        ),
    )(*rows, gate_weight, up_weight, down_weight)


def unpack(packed):
    count = packed.shape[0]
    columns = packed.shape[1] // CAP
    main = packed[:, : columns * MAIN].reshape(count, columns, MAIN, 128)
    main = main.transpose(0, 2, 1, 3).reshape(count * MAIN, columns * 128)
    last = packed[:, columns * MAIN :].reshape(count, columns * 128)
    return jnp.concatenate([main, last], axis=0)


def pack(rows):
    count = rows.shape[0] // CAP
    columns = rows.shape[1] // 128
    main = rows[: count * MAIN].reshape(count, MAIN, columns, 128)
    main = main.transpose(0, 2, 1, 3).reshape(count, columns * MAIN, 128)
    last = rows[count * MAIN :].reshape(count, columns, 128)
    return jnp.concatenate([main, last], axis=1)


def swap_experts(packed):
    return lax.all_to_all(packed, "ep", 0, 0, tiled=True)


def expert_rows(arrived, weights):
    half = arrived.shape[0] // 2
    rows0, rows1 = unpack(arrived[:half]), unpack(arrived[half:])
    right0 = shift_tp(rows0, 1)
    left1 = shift_tp(rows1, 3)
    far0 = shift_tp(right0, 1)
    far1 = shift_tp(left1, 3)
    right1 = shift_tp(rows1, 1)
    left0 = shift_tp(rows0, 3)
    own0, own1 = expert([rows0, rows1], *weights)
    p_right0, p_left1 = expert([right0, left1], *weights)
    p_far0, p_far1 = expert([far0, far1], *weights)
    p_right1, p_left0 = expert([right1, left0], *weights)
    from1_1 = shift_tp(p_left1, 1)
    from3_0 = shift_tp(p_right0, 3)
    via0 = shift_tp(p_far0, 1)
    via1 = shift_tp(p_far1, 3)
    from1_0 = shift_tp((p_left0.astype(F32) + via0.astype(F32)).astype(BF16), 1)
    from3_1 = shift_tp((p_right1.astype(F32) + via1.astype(F32)).astype(BF16), 3)
    low = own0.astype(F32) + from1_0.astype(F32) + from3_0.astype(F32)
    high = own1.astype(F32) + from1_1.astype(F32) + from3_1.astype(F32)
    return jnp.concatenate([pack(low.astype(BF16)), pack(high.astype(BF16))])


def body(
    query_rows,
    key_rows,
    value_rows,
    sink_logit,
    out_weight,
    routed_rows,
    norm_gain,
    routing,
    route_weight,
    gate_weight,
    up_weight,
    down_weight,
):
    experts = lax.axis_size("ep")
    fetched = fetch_weight(out_weight)
    sent = dispatch(routed_rows, norm_gain, routing, route_weight, experts)
    attended = attention(query_rows, key_rows, value_rows, sink_logit)
    mixed = mix_tokens(attended, out_weight, fetched)
    weights = (gate_weight[0], up_weight[0], down_weight[0])
    out, high, low = sent
    arrived = swap_experts(out)
    summed = expert_rows(arrived, weights)
    back = unpack(swap_experts(summed))
    rows = ((0,), (0,))
    return mixed, (dot(high, back, rows) + dot(low, back, rows)).astype(BF16)


def solution(mesh):
    in_specs = (
        P("ep", "tp"),
        P("ep", "tp"),
        P("ep", "tp"),
        P("tp"),
        P("tp", None),
        P(("ep", "tp"), None),
        P(),
        P(("ep", "tp"), None),
        P(("ep", "tp"), None),
        P("ep", None, "tp"),
        P("ep", None, "tp"),
        P("ep", "tp", None),
    )
    out_specs = (P(("ep", "tp"), None), P(("ep", "tp"), None))
    return jax.shard_map(body, mesh=mesh, in_specs=in_specs, out_specs=out_specs, check_vma=False)
```

time: 273 us -> 201 us (0.74)
  blocking collectives: 94.7 us -> 0 us
  Pallas kernels: 0 us -> 76.4 us
  matrix products: 57.8 us -> 1.74 us
  starting transfers between devices: 11.2 us -> 48.8 us
  local copies, waits for them, and re-layouts: 30.2 us -> 7.39 us
  between operations: 14.3 us -> 1.12 us
  waiting for transfers between devices: 46.4 us -> 57.3 us
  other arithmetic: 15.8 us -> 7.44 us
    all_to_all x2 -> x0, blocking collectives: 94.7 us -> none  [the longest x1 58 us: sum_at_owner(): pieces = lax.all_to_all(split_up(value, dim, peers), axis, 0, 0, tiled=True)]
    pallas_call x0 -> x7, Pallas kernels: none -> 76.4 us  [the longest x4 60.3 us: expert(): pl.pallas_call(functools.partial(expert_kernel, pieces=pieces), grid=(uni...]
    dot_general x7 -> x2, matrix products: 57.8 us -> 1.74 us  [dot(): return lax.dot_general(a, b, (dims, ((), ())), preferred_element_type=F32)]
    ppermute x2 -> x23, waiting for transfers between devices: 1.68 us -> 47.8 us  [the longest x18 47.8 us: shift_tp(): return lax.ppermute(value, 'tp', ring(shift))]
    ppermute x2 -> x23, starting transfers between devices: 3.49 us -> 33.1 us  [the longest x18 28.9 us: shift_tp(): return lax.ppermute(value, 'tp', ring(shift))]
    all_to_all x1 -> x2, waiting for transfers between devices: 29.6 us -> 9.59 us  [swap_experts(): return lax.all_to_all(packed, 'ep', 0, 0, tiled=True)]
    all_gather x1 -> x0, waiting for transfers between devices: 15 us -> none  [expert_sectioned(): lax.all_gather(arrived, 'tp', axis=0, tiled=True)]
    reduce_sum x6 -> x0, other arithmetic: 11.3 us -> none  [the longest x1 3.93 us: body(): jnp.sum(picked.reshape(token_count, top_count, model_width), axis=1)]
  transfers between devices with their start and end apart: 5 -> 25, of which waited for: 3 -> 8; matrix products, arithmetic and copies ran while one was open for 31% -> 6% of each run, Pallas kernels for 0% -> 37%
where the time goes in v1:
time: 201 us; the launch traced here: 200 us
  Pallas kernels  76.4 us (38%)
  waiting for transfers between devices  57.3 us (29%)
  starting transfers between devices  48.8 us (24%)
  other arithmetic  7.44 us (4%)
  local copies, waits for them, and re-layouts  7.39 us (4%)
    pallas_call x4, Pallas kernels, expert(): pl.pallas_call(functools.partial(expert_kernel, pieces=pieces), grid=(uni...  60.3 us
    ppermute x18, waiting for transfers between devices, shift_tp(): return lax.ppermute(value, 'tp', ring(shift))  47.8 us
    ppermute x18, starting transfers between devices, shift_tp(): return lax.ppermute(value, 'tp', ring(shift))  28.9 us
    all_to_all x2, starting transfers between devices, swap_experts(): return lax.all_to_all(packed, 'ep', 0, 0, tiled=True)  15.7 us
    all_to_all x2, waiting for transfers between devices, swap_experts(): return lax.all_to_all(packed, 'ep', 0, 0, tiled=True)  9.59 us
    pallas_call x1, Pallas kernels, attention(): pl.pallas_call(attention_kernel, grid=(rows // WINDOW,), in_specs=[pl.Blo...  7.54 us
    pallas_call x1, Pallas kernels, project(): pl.pallas_call(project_kernel, grid=(width // step,), in_specs=[pl.BlockS...  5.54 us
  transfers between devices with their start and end apart: 25, of which 8 were waited for; matrix products, arithmetic and copies ran while one was open for 6% of the time, Pallas kernels for 37%

profile of v1, /device:TPU:0, one launch (start us, length us, event | category | flops | bytes accessed | tf_op | source)
XLA Modules:
  0.0 200.2 jit_solution(10777284740833910362)
XLA Ops:
  0.6 3.0 %dispatch.1 = (bf16[32,144,128]{2,1,0:T(8,128)(2,1)}, bf16[288,128]{1,0:T(8,128)(2,1)}, bf16[288,128]{1,0:T(8,128)(2,1)}) custom-call(bf16[128,2048]{1,0:T(8,128)(2,1)} %rows_ref.1, f32[1,2048]{1,0:T(1,128)} %bitcast.79, s32[2,128]{1,0:T(2,128)} %bitcast.80, f32[2,128]{1,0:T(2,128)} %bitcast.81), custom_call_target="tpu_custom_call" | custom-call | flops 400000000 | bytes 2500000 | tf_op jit(solution)/shard_map/dispatch/pallas_call | solution.py:69
  3.6 8.6 %all-to-all-start = ((bf16[32,144,128]{2,1,0:T(8,128)(2,1)}), bf16[32,144,128]{2,1,0:T(8,128)(2,1)S(1)}, u32[]{:S(2)}, u32[]{:S(2)}) async-start(bf16[32,144,128]{2,1,0:T(8,128)(2,1)} %get-tuple-element.14), calls=%async_computation | async-start | bytes 2359296 | tf_op jit(solution)/shard_map/all_to_all | solution.py:298
  12.3 3.1 %collective-permute-start.9 = (bf16[128,2048]{1,0:T(8,128)(2,1)S(1)}, bf16[128,2048]{1,0:T(8,128)(2,1)}, u32[]{:S(2)}, u32[]{:S(2)}) collective-permute-start(bf16[128,2048]{1,0:T(8,128)(2,1)S(1)} %constant_dynamic-slice_fusion), channel_id=1, source_target_pairs={{0,2},{1,3},{2,0},{3,1},{4,6},{5,7},{6,4},{7,5},{8,10},{9,11},{10,... | collective-permute-start | bytes 1572872 | tf_op jit(solution)/shard_map/ppermute | solution.py:160
  17.1 2.2 %collective-permute-start = (bf16[128,128]{1,0:T(8,128)(2,1)}, bf16[128,128]{1,0:T(8,128)(2,1)}, u32[]{:S(2)}, u32[]{:S(2)}) collective-permute-start(bf16[128,128]{1,0:T(8,128)(2,1)} %get-tuple-element.32), channel_id=1, source_target_pairs={{0,4},{4,8},{8,12},{12,16},{16,20},{20,24},{24,28},{28,32},{32,36}... | collective-permute-start | bytes 98312 | tf_op jit(solution)/shard_map/ppermute | solution.py:130
  21.3 9.6 %all-to-all-done = bf16[32,144,128]{2,1,0:T(8,128)(2,1)S(1)} async-done(((bf16[32,144,128]{2,1,0:T(8,128)(2,1)}), bf16[32,144,128]{2,1,0:T(8,128)(2,1)S(1)}, u32[]{:S(2)}, u32[]{:S(2)}) %all-to-all-start) | async-done | bytes 1179680 | tf_op jit(solution)/shard_map/all_to_all | solution.py:298
  36.0 16.0 %collective-permute-done.13.refs_0_ = bf16[144,2048]{1,0:T(8,128)(2,1)} collective-permute-done((bf16[144,2048]{1,0:T(8,128)(2,1)S(1)}, bf16[144,2048]{1,0:T(8,128)(2,1)}, u32[]{:S(2)}, u32[]{:S(2)}) %collective-permute-start.13) | collective-permute-done | bytes 589856 | tf_op jit(solution)/shard_map/ppermute | solution.py:160
  52.0 2.2 %collective-permute-start.14 = (bf16[144,2048]{1,0:T(8,128)(2,1)}, bf16[144,2048]{1,0:T(8,128)(2,1)}, u32[]{:S(2)}, u32[]{:S(2)}) collective-permute-start(bf16[144,2048]{1,0:T(8,128)(2,1)} %collective-permute-done.13.refs_0_), channel_id=1, source_target_pairs={{0,1},{1,2},{2,3},{3,0},{4,5},{5,6},{6,7},{7,4},{8,9},{9,10},{10,1... | collective-permute-start | bytes 1769480 | tf_op jit(solution)/shard_map/ppermute | solution.py:160
  55.3 15.1 %expert.7 = (bf16[144,2048]{1,0:T(8,128)(2,1)}, bf16[144,2048]{1,0:T(8,128)(2,1)}) custom-call(bf16[144,2048]{1,0:T(8,128)(2,1)} %collective-permute-done.13.refs_0_, bf16[144,2048]{1,0:T(8,128)(2,1)} %collective-permute-done.15.refs_1_, bf16[2048,1792]{1,0:T(8,128)(2,1)} %bitcast.67, bf16[2048,1792]{1,0:T(8,128)(2,1)} %bitcast.71, bf16[1792,2048]{1,0:T(8,128)(2,1)} %bitcast.75), custom_call_target="tpu_custom_call" | custom-call | flops 6341787648 | bytes 22020096 | tf_op jit(solution)/shard_map/expert/pallas_call | solution.py:260
  70.4 6.8 %collective-permute-done.14.refs_0_ = bf16[144,2048]{1,0:T(8,128)(2,1)} collective-permute-done((bf16[144,2048]{1,0:T(8,128)(2,1)}, bf16[144,2048]{1,0:T(8,128)(2,1)}, u32[]{:S(2)}, u32[]{:S(2)}) %collective-permute-start.14) | collective-permute-done | bytes 589856 | tf_op jit(solution)/shard_map/ppermute | solution.py:160
  77.8 2.1 %collective-permute-start.19 = (bf16[144,2048]{1,0:T(8,128)(2,1)}, bf16[144,2048]{1,0:T(8,128)(2,1)}, u32[]{:S(2)}, u32[]{:S(2)}) collective-permute-start(bf16[144,2048]{1,0:T(8,128)(2,1)} %get-tuple-element.18), channel_id=1, source_target_pairs={{0,3},{1,0},{2,1},{3,2},{4,7},{5,4},{6,5},{7,6},{8,11},{9,8},{10,9... | collective-permute-start | bytes 1769480 | tf_op jit(solution)/shard_map/ppermute | solution.py:160
  80.0 15.0 %expert.6 = (bf16[144,2048]{1,0:T(8,128)(2,1)}, bf16[144,2048]{1,0:T(8,128)(2,1)}) custom-call(bf16[144,2048]{1,0:T(8,128)(2,1)} %collective-permute-done.14.refs_0_, bf16[144,2048]{1,0:T(8,128)(2,1)} %collective-permute-done.16.refs_1_, bf16[2048,1792]{1,0:T(8,128)(2,1)} %bitcast.68, bf16[2048,1792]{1,0:T(8,128)(2,1)} %bitcast.72, bf16[1792,2048]{1,0:T(8,128)(2,1)} %bitcast.76), custom_call_target="tpu_custom_call" | custom-call | flops 6341787648 | bytes 22020096 | tf_op jit(solution)/shard_map/expert/pallas_call | solution.py:260
  95.8 15.1 %expert.5 = (bf16[144,2048]{1,0:T(8,128)(2,1)}, bf16[144,2048]{1,0:T(8,128)(2,1)}) custom-call(bf16[144,2048]{1,0:T(8,128)(2,1)} %copy-done.15, bf16[144,2048]{1,0:T(8,128)(2,1)} %collective-permute-done.12.refs_1_, bf16[2048,1792]{1,0:T(8,128)(2,1)} %bitcast.69, bf16[2048,1792]{1,0:T(8,128)(2,1)} %bitcast.73, bf16[1792,2048]{1,0:T(8,128)(2,1)} %bitcast.77), custom_call_target="tpu_custom_call" | custom-call | flops 6341787648 | bytes 22020096 | tf_op jit(solution)/shard_map/expert/pallas_call | solution.py:260
  110.9 3.2 %collective-permute-start.21 = (bf16[144,2048]{1,0:T(8,128)(2,1)}, bf16[144,2048]{1,0:T(8,128)(2,1)S(1)}, u32[]{:S(2)}, u32[]{:S(2)}) collective-permute-start(bf16[144,2048]{1,0:T(8,128)(2,1)} %get-tuple-element.22), channel_id=1, source_target_pairs={{0,3},{1,0},{2,1},{3,2},{4,7},{5,4},{6,5},{7,6},{8,11},{9,8},{10,9... | collective-permute-start | bytes 1769480 | tf_op jit(solution)/shard_map/ppermute | solution.py:160
  115.6 15.1 %expert.4 = (bf16[144,2048]{1,0:T(8,128)(2,1)}, bf16[144,2048]{1,0:T(8,128)(2,1)}) custom-call(bf16[144,2048]{1,0:T(8,128)(2,1)} %copy-done.3, bf16[144,2048]{1,0:T(8,128)(2,1)} %copy-done.4, bf16[2048,1792]{1,0:T(8,128)(2,1)} %bitcast.70, bf16[2048,1792]{1,0:T(8,128)(2,1)} %bitcast.74, bf16[1792,2048]{1,0:T(8,128)(2,1)} %bitcast.78), custom_call_target="tpu_custom_call" | custom-call | flops 6341787648 | bytes 22020096 | tf_op jit(solution)/shard_map/expert/pallas_call | solution.py:260
  130.7 3.3 %collective-permute-start.7 = (bf16[128,2048]{1,0:T(8,128)(2,1)S(1)}, bf16[128,2048]{1,0:T(8,128)(2,1)}, u32[]{:S(2)}, u32[]{:S(2)}) collective-permute-start(bf16[128,2048]{1,0:T(8,128)(2,1)S(1)} %constant_dynamic-slice_fusion), channel_id=1, source_target_pairs={{0,3},{1,0},{2,1},{3,2},{4,7},{5,4},{6,5},{7,6},{8,11},{9,8},{10,9... | collective-permute-start | bytes 1572872 | tf_op jit(solution)/shard_map/ppermute | solution.py:160
  134.3 3.2 %collective-permute-start.22 = (bf16[144,2048]{1,0:T(8,128)(2,1)S(1)}, bf16[144,2048]{1,0:T(8,128)(2,1)S(1)}, u32[]{:S(2)}, u32[]{:S(2)}) collective-permute-start(bf16[144,2048]{1,0:T(8,128)(2,1)S(1)} %add_convert_fusion.1), channel_id=1, source_target_pairs={{0,3},{1,0},{2,1},{3,2},{4,7},{5,4},{6,5},{7,6},{8,11},{9,8},{10,9... | collective-permute-start | bytes 1769480 | tf_op jit(solution)/shard_map/ppermute | solution.py:160
  138.9 9.5 %collective-permute-done.20 = bf16[144,2048]{1,0:T(8,128)(2,1)S(1)} collective-permute-done((bf16[144,2048]{1,0:T(8,128)(2,1)S(1)}, bf16[144,2048]{1,0:T(8,128)(2,1)S(1)}, u32[]{:S(2)}, u32[]{:S(2)}) %collective-permute-start.20) | collective-permute-done | bytes 589856 | tf_op jit(solution)/shard_map/ppermute | solution.py:160
  148.4 7.6 %collective-permute-done.22 = bf16[144,2048]{1,0:T(8,128)(2,1)S(1)} collective-permute-done((bf16[144,2048]{1,0:T(8,128)(2,1)S(1)}, bf16[144,2048]{1,0:T(8,128)(2,1)S(1)}, u32[]{:S(2)}, u32[]{:S(2)}) %collective-permute-start.22) | collective-permute-done | bytes 589856 | tf_op jit(solution)/shard_map/ppermute | solution.py:160
  157.6 7.1 %all-to-all-start.1 = ((bf16[32,144,128]{2,1,0:T(8,128)(2,1)}), bf16[32,144,128]{2,1,0:T(8,128)(2,1)S(1)}, u32[]{:S(2)}, u32[]{:S(2)}) async-start(bf16[32,144,128]{2,1,0:T(8,128)(2,1)} %maximum_maximum_fusion), calls=%async_computation.1 | async-start | bytes 2359296 | tf_op jit(solution)/shard_map/all_to_all | solution.py:298
  165.6 7.5 %attention.1 = bf16[1024,256]{1,0:T(8,128)(2,1)} custom-call(s32[2]{0:T(128)} %add_convert_fusion.4.edge_ref, f32[4]{0:T(128)} %sink_ref.1, bf16[1024,256]{1,0:T(8,128)(2,1)} %query_ref.1, bf16[1280,128]{1,0:T(8,128)(2,1)} %copy-done, bf16[1280,128]{1,0:T(8,128)(2,1)} %pad_maximum_fusion.6.vk_ref), custom_call_target="tpu_custom_call" | custom-call | flops 4000000000 | bytes 2000000 | tf_op jit(solution)/shard_map/attention/pallas_call | solution.py:137
  175.7 2.2 %collective-permute-start.4 = (bf16[256,256]{1,0:T(8,128)(2,1)S(1)}, bf16[256,256]{1,0:T(8,128)(2,1)S(1)}, u32[]{:S(2)}, u32[]{:S(2)}) collective-permute-start(bf16[256,256]{1,0:T(8,128)(2,1)S(1)} %get-tuple-element.28), channel_id=1, source_target_pairs={{0,2},{1,3},{2,0},{3,1},{4,6},{5,7},{6,4},{7,5},{8,10},{9,11},{10,... | collective-permute-start | bytes 393224 | tf_op jit(solution)/shard_map/ppermute | solution.py:160
  179.4 3.4 %collective-permute-done.4 = bf16[256,256]{1,0:T(8,128)(2,1)S(1)} collective-permute-done((bf16[256,256]{1,0:T(8,128)(2,1)S(1)}, bf16[256,256]{1,0:T(8,128)(2,1)S(1)}, u32[]{:S(2)}, u32[]{:S(2)}) %collective-permute-start.4) | collective-permute-done | bytes 131104 | tf_op jit(solution)/shard_map/ppermute | solution.py:160
  187.4 2.9 %collective-permute-done.2 = bf16[256,256]{1,0:T(8,128)(2,1)S(1)} collective-permute-done((bf16[256,256]{1,0:T(8,128)(2,1)S(1)}, bf16[256,256]{1,0:T(8,128)(2,1)S(1)}, u32[]{:S(2)}, u32[]{:S(2)}) %collective-permute-start.2) | collective-permute-done | bytes 131104 | tf_op jit(solution)/shard_map/ppermute | solution.py:160
  192.0 5.5 %project.1 = bf16[256,2048]{1,0:T(8,128)(2,1)} custom-call(bf16[256,256]{1,0:T(8,128)(2,1)} %get-tuple-element.31.refs_0_, bf16[256,128]{1,0:T(8,128)(2,1)} %get-tuple-element.41.refs_1_, bf16[256,128]{1,0:T(8,128)(2,1)} %get-tuple-element.40.refs_2_, bf16[256,128]{1,0:T(8,128)(2,1)} %get-tuple-element.39.refs_3_, ...), custom_call_target="tpu_custom_call" | custom-call | flops 1100000000 | bytes 6000000 | tf_op jit(solution)/shard_map/project/pallas_call | solution.py:176
  (99 shorter events, 29.7 us)
Async XLA Ops:
  3.6 27.3 %all-to-all-start = ((bf16[32,144,128]{2,1,0:T(8,128)(2,1)}), bf16[32,144,128]{2,1,0:T(8,128)(2,1)S(1)}, u32[]{:S(2)}, u32[]{:S(2)}) async-start(bf16[32,144,128]{2,1,0:T(8,128)(2,1)} %get-tuple-element.14), calls=%async_computation | async-start | bytes 2359296 | tf_op jit(solution)/shard_map/all_to_all | solution.py:298
  12.3 160.8 %collective-permute-start.9 = (bf16[128,2048]{1,0:T(8,128)(2,1)S(1)}, bf16[128,2048]{1,0:T(8,128)(2,1)}, u32[]{:S(2)}, u32[]{:S(2)}) collective-permute-start(bf16[128,2048]{1,0:T(8,128)(2,1)S(1)} %constant_dynamic-slice_fusion), channel_id=1, source_target_pairs={{0,2},{1,3},{2,0},{3,1},{4,6},{5,7},{6,4},{7,5},{8,10},{9,11},{10,... | collective-permute-start | bytes 1572872 | tf_op jit(solution)/shard_map/ppermute | solution.py:160
  15.4 158.0 %collective-permute-start.5 = (bf16[128,2048]{1,0:T(8,128)(2,1)S(1)}, bf16[128,2048]{1,0:T(8,128)(2,1)}, u32[]{:S(2)}, u32[]{:S(2)}) collective-permute-start(bf16[128,2048]{1,0:T(8,128)(2,1)S(1)} %constant_dynamic-slice_fusion), channel_id=1, source_target_pairs={{0,1},{1,2},{2,3},{3,0},{4,5},{5,6},{6,7},{7,4},{8,9},{9,10},{10,1... | collective-permute-start | bytes 1572872 | tf_op jit(solution)/shard_map/ppermute | solution.py:160
  17.1 15.7 %collective-permute-start = (bf16[128,128]{1,0:T(8,128)(2,1)}, bf16[128,128]{1,0:T(8,128)(2,1)}, u32[]{:S(2)}, u32[]{:S(2)}) collective-permute-start(bf16[128,128]{1,0:T(8,128)(2,1)} %get-tuple-element.32), channel_id=1, source_target_pairs={{0,4},{4,8},{8,12},{12,16},{16,20},{20,24},{24,28},{28,32},{32,36}... | collective-permute-start | bytes 98312 | tf_op jit(solution)/shard_map/ppermute | solution.py:130
  19.3 15.3 %collective-permute-start.1 = (bf16[128,128]{1,0:T(8,128)(2,1)}, bf16[128,128]{1,0:T(8,128)(2,1)}, u32[]{:S(2)}, u32[]{:S(2)}) collective-permute-start(bf16[128,128]{1,0:T(8,128)(2,1)} %get-tuple-element.33), channel_id=1, source_target_pairs={{4,0},{8,4},{12,8},{16,12},{20,16},{24,20},{28,24},{32,28},{36,32}... | collective-permute-start | bytes 98312 | tf_op jit(solution)/shard_map/ppermute | solution.py:131
  31.1 20.9 %collective-permute-start.13 = (bf16[144,2048]{1,0:T(8,128)(2,1)S(1)}, bf16[144,2048]{1,0:T(8,128)(2,1)}, u32[]{:S(2)}, u32[]{:S(2)}) collective-permute-start(bf16[144,2048]{1,0:T(8,128)(2,1)S(1)} %pad_maximum_fusion.3.refs_0_), channel_id=1, source_target_pairs={{0,1},{1,2},{2,3},{3,0},{4,5},{5,6},{6,7},{7,4},{8,9},{9,10},{10,1... | collective-permute-start | bytes 1769480 | tf_op jit(solution)/shard_map/ppermute | solution.py:160
  32.8 21.4 %collective-permute-start.15 = (bf16[144,2048]{1,0:T(8,128)(2,1)S(1)}, bf16[144,2048]{1,0:T(8,128)(2,1)}, u32[]{:S(2)}, u32[]{:S(2)}) collective-permute-start(bf16[144,2048]{1,0:T(8,128)(2,1)S(1)} %pad_maximum_fusion.4.refs_1_), channel_id=1, source_target_pairs={{0,3},{1,0},{2,1},{3,2},{4,7},{5,4},{6,5},{7,6},{8,11},{9,8},{10,9... | collective-permute-start | bytes 1769480 | tf_op jit(solution)/shard_map/ppermute | solution.py:160
  35.7 59.3 %collective-permute-start.11 = (bf16[144,2048]{1,0:T(8,128)(2,1)S(1)}, bf16[144,2048]{1,0:T(8,128)(2,1)S(1)}, u32[]{:S(2)}, u32[]{:S(2)}) collective-permute-start(bf16[144,2048]{1,0:T(8,128)(2,1)S(1)} %pad_maximum_fusion.4.refs_1_), channel_id=1, source_target_pairs={{0,1},{1,2},{2,3},{3,0},{4,5},{5,6},{6,7},{7,4},{8,9},{9,10},{10,1... | collective-permute-start | bytes 1769480 | tf_op jit(solution)/shard_map/ppermute | solution.py:160
  52.0 25.2 %collective-permute-start.14 = (bf16[144,2048]{1,0:T(8,128)(2,1)}, bf16[144,2048]{1,0:T(8,128)(2,1)}, u32[]{:S(2)}, u32[]{:S(2)}) collective-permute-start(bf16[144,2048]{1,0:T(8,128)(2,1)} %collective-permute-done.13.refs_0_), channel_id=1, source_target_pairs={{0,1},{1,2},{2,3},{3,0},{4,5},{5,6},{6,7},{7,4},{8,9},{9,10},{10,1... | collective-permute-start | bytes 1769480 | tf_op jit(solution)/shard_map/ppermute | solution.py:160
  54.2 23.6 %collective-permute-start.16 = (bf16[144,2048]{1,0:T(8,128)(2,1)}, bf16[144,2048]{1,0:T(8,128)(2,1)}, u32[]{:S(2)}, u32[]{:S(2)}) collective-permute-start(bf16[144,2048]{1,0:T(8,128)(2,1)} %collective-permute-done.15.refs_1_), channel_id=1, source_target_pairs={{0,3},{1,0},{2,1},{3,2},{4,7},{5,4},{6,5},{7,6},{8,11},{9,8},{10,9... | collective-permute-start | bytes 1769480 | tf_op jit(solution)/shard_map/ppermute | solution.py:160
  77.2 18.6 %collective-permute-start.12 = (bf16[144,2048]{1,0:T(8,128)(2,1)S(1)}, bf16[144,2048]{1,0:T(8,128)(2,1)}, u32[]{:S(2)}, u32[]{:S(2)}) collective-permute-start(bf16[144,2048]{1,0:T(8,128)(2,1)S(1)} %pad_maximum_fusion.3.refs_0_), channel_id=1, source_target_pairs={{0,3},{1,0},{2,1},{3,2},{4,7},{5,4},{6,5},{7,6},{8,11},{9,8},{10,9... | collective-permute-start | bytes 1769480 | tf_op jit(solution)/shard_map/ppermute | solution.py:160
  77.8 56.3 %collective-permute-start.19 = (bf16[144,2048]{1,0:T(8,128)(2,1)}, bf16[144,2048]{1,0:T(8,128)(2,1)}, u32[]{:S(2)}, u32[]{:S(2)}) collective-permute-start(bf16[144,2048]{1,0:T(8,128)(2,1)} %get-tuple-element.18), channel_id=1, source_target_pairs={{0,3},{1,0},{2,1},{3,2},{4,7},{5,4},{6,5},{7,6},{8,11},{9,8},{10,9... | collective-permute-start | bytes 1769480 | tf_op jit(solution)/shard_map/ppermute | solution.py:160
  95.8 18.3 %collective-permute-start.17 = (bf16[144,2048]{1,0:T(8,128)(2,1)}, bf16[144,2048]{1,0:T(8,128)(2,1)S(1)}, u32[]{:S(2)}, u32[]{:S(2)}) collective-permute-start(bf16[144,2048]{1,0:T(8,128)(2,1)} %get-tuple-element.17), channel_id=1, source_target_pairs={{0,1},{1,2},{2,3},{3,0},{4,5},{5,6},{6,7},{7,4},{8,9},{9,10},{10,1... | collective-permute-start | bytes 1769480 | tf_op jit(solution)/shard_map/ppermute | solution.py:160
  110.9 19.8 %collective-permute-start.21 = (bf16[144,2048]{1,0:T(8,128)(2,1)}, bf16[144,2048]{1,0:T(8,128)(2,1)S(1)}, u32[]{:S(2)}, u32[]{:S(2)}) collective-permute-start(bf16[144,2048]{1,0:T(8,128)(2,1)} %get-tuple-element.22), channel_id=1, source_target_pairs={{0,3},{1,0},{2,1},{3,2},{4,7},{5,4},{6,5},{7,6},{8,11},{9,8},{10,9... | collective-permute-start | bytes 1769480 | tf_op jit(solution)/shard_map/ppermute | solution.py:160
  115.4 18.9 %collective-permute-start.18 = (bf16[144,2048]{1,0:T(8,128)(2,1)S(1)}, bf16[144,2048]{1,0:T(8,128)(2,1)S(1)}, u32[]{:S(2)}, u32[]{:S(2)}) collective-permute-start(bf16[144,2048]{1,0:T(8,128)(2,1)S(1)} %add_convert_fusion.3), channel_id=1, source_target_pairs={{0,1},{1,2},{2,3},{3,0},{4,5},{5,6},{6,7},{7,4},{8,9},{9,10},{10,1... | collective-permute-start | bytes 1769480 | tf_op jit(solution)/shard_map/ppermute | solution.py:160
  130.7 42.9 %collective-permute-start.7 = (bf16[128,2048]{1,0:T(8,128)(2,1)S(1)}, bf16[128,2048]{1,0:T(8,128)(2,1)}, u32[]{:S(2)}, u32[]{:S(2)}) collective-permute-start(bf16[128,2048]{1,0:T(8,128)(2,1)S(1)} %constant_dynamic-slice_fusion), channel_id=1, source_target_pairs={{0,3},{1,0},{2,1},{3,2},{4,7},{5,4},{6,5},{7,6},{8,11},{9,8},{10,9... | collective-permute-start | bytes 1572872 | tf_op jit(solution)/shard_map/ppermute | solution.py:160
  134.2 14.3 %collective-permute-start.20 = (bf16[144,2048]{1,0:T(8,128)(2,1)S(1)}, bf16[144,2048]{1,0:T(8,128)(2,1)S(1)}, u32[]{:S(2)}, u32[]{:S(2)}) collective-permute-start(bf16[144,2048]{1,0:T(8,128)(2,1)S(1)} %copy-done.14), channel_id=1, source_target_pairs={{0,1},{1,2},{2,3},{3,0},{4,5},{5,6},{6,7},{7,4},{8,9},{9,10},{10,1... | collective-permute-start | bytes 1769480 | tf_op jit(solution)/shard_map/ppermute | solution.py:160
  134.3 21.7 %collective-permute-start.22 = (bf16[144,2048]{1,0:T(8,128)(2,1)S(1)}, bf16[144,2048]{1,0:T(8,128)(2,1)S(1)}, u32[]{:S(2)}, u32[]{:S(2)}) collective-permute-start(bf16[144,2048]{1,0:T(8,128)(2,1)S(1)} %add_convert_fusion.1), channel_id=1, source_target_pairs={{0,3},{1,0},{2,1},{3,2},{4,7},{5,4},{6,5},{7,6},{8,11},{9,8},{10,9... | collective-permute-start | bytes 1769480 | tf_op jit(solution)/shard_map/ppermute | solution.py:160
  157.6 40.0 %all-to-all-start.1 = ((bf16[32,144,128]{2,1,0:T(8,128)(2,1)}), bf16[32,144,128]{2,1,0:T(8,128)(2,1)S(1)}, u32[]{:S(2)}, u32[]{:S(2)}) async-start(bf16[32,144,128]{2,1,0:T(8,128)(2,1)} %maximum_maximum_fusion), calls=%async_computation.1 | async-start | bytes 2359296 | tf_op jit(solution)/shard_map/all_to_all | solution.py:298
  173.1 17.8 %collective-permute-start.10 = (bf16[128,2048]{1,0:T(8,128)(2,1)}, bf16[128,2048]{1,0:T(8,128)(2,1)S(1)}, u32[]{:S(2)}, u32[]{:S(2)}) collective-permute-start(bf16[128,2048]{1,0:T(8,128)(2,1)} %collective-permute-done.9.refs_12_), channel_id=1, source_target_pairs={{0,4},{4,0},{8,12},{12,8},{16,20},{20,16},{24,28},{28,24},{32,36},... | collective-permute-start | bytes 1572872 | tf_op jit(solution)/shard_map/ppermute | solution.py:197
  173.4 17.5 %collective-permute-start.6 = (bf16[128,2048]{1,0:T(8,128)(2,1)}, bf16[128,2048]{1,0:T(8,128)(2,1)S(1)}, u32[]{:S(2)}, u32[]{:S(2)}) collective-permute-start(bf16[128,2048]{1,0:T(8,128)(2,1)} %collective-permute-done.5.refs_8_), channel_id=1, source_target_pairs={{0,4},{4,0},{8,12},{12,8},{16,20},{20,16},{24,28},{28,24},{32,36},... | collective-permute-start | bytes 1572872 | tf_op jit(solution)/shard_map/ppermute | solution.py:197
  173.6 17.3 %collective-permute-start.8 = (bf16[128,2048]{1,0:T(8,128)(2,1)}, bf16[128,2048]{1,0:T(8,128)(2,1)S(1)}, u32[]{:S(2)}, u32[]{:S(2)}) collective-permute-start(bf16[128,2048]{1,0:T(8,128)(2,1)} %collective-permute-done.7.refs_10_), channel_id=1, source_target_pairs={{0,4},{4,0},{8,12},{12,8},{16,20},{20,16},{24,28},{28,24},{32,36},... | collective-permute-start | bytes 1572872 | tf_op jit(solution)/shard_map/ppermute | solution.py:197
  177.9 8.8 %collective-permute-start.3 = (bf16[256,256]{1,0:T(8,128)(2,1)S(1)}, bf16[256,256]{1,0:T(8,128)(2,1)S(1)}, u32[]{:S(2)}, u32[]{:S(2)}) collective-permute-start(bf16[256,256]{1,0:T(8,128)(2,1)S(1)} %get-tuple-element.29), channel_id=1, source_target_pairs={{0,3},{1,0},{2,1},{3,2},{4,7},{5,4},{6,5},{7,6},{8,11},{9,8},{10,9... | collective-permute-start | bytes 393224 | tf_op jit(solution)/shard_map/ppermute | solution.py:160
  182.8 7.4 %collective-permute-start.2 = (bf16[256,256]{1,0:T(8,128)(2,1)S(1)}, bf16[256,256]{1,0:T(8,128)(2,1)S(1)}, u32[]{:S(2)}, u32[]{:S(2)}) collective-permute-start(bf16[256,256]{1,0:T(8,128)(2,1)S(1)} %get-tuple-element.30), channel_id=1, source_target_pairs={{0,1},{1,2},{2,3},{3,0},{4,5},{5,6},{6,7},{7,4},{8,9},{9,10},{10,1... | collective-permute-start | bytes 393224 | tf_op jit(solution)/shard_map/ppermute | solution.py:160
  (17 other events, 202.5 us)

commit v2 on v1

--- a/solution.py
+++ b/solution.py
@@ -120,15 +120,21 @@
         out_ref[:, lanes] = (total[:, : 2 * HEAD_DIM] / denominator).astype(BF16)
 
 
-def attention(query_rows, key_rows, value_rows, sink_logit):
+def halo_rows(key_rows, value_rows):
     peers = lax.axis_size("ep")
-    me = lax.axis_index("ep")
     up = [(i, i + 1) for i in range(peers - 1)]
     down = [(j, i) for i, j in up]
     joined = jnp.concatenate([key_rows, value_rows], axis=1)
     rows = joined.shape[0]
     before = lax.ppermute(joined[rows - WINDOW :], "ep", up)
     after = lax.ppermute(joined[:WINDOW], "ep", down)
+    return before, joined, after
+
+
+def attention(query_rows, before, joined, after, sink_logit):
+    peers = lax.axis_size("ep")
+    me = lax.axis_index("ep")
+    rows = joined.shape[0]
     kv = jnp.concatenate([before, joined, after], axis=0)
     vk = jnp.concatenate([kv[:, HEAD_DIM:], kv[:, :HEAD_DIM]], axis=1)
     edge = jnp.stack([me == 0, me == peers - 1]).astype(jnp.int32)
@@ -147,6 +153,7 @@
         out_specs=pl.BlockSpec((WINDOW, width), lambda i: (i, 0)),
         out_shape=jax.ShapeDtypeStruct((rows, width), BF16),
         name="attention",
+        compiler_params=pltpu.CompilerParams(vmem_limit_bytes=20 * 1024 * 1024),
         cost_estimate=pl.CostEstimate(flops=4_000_000_000, transcendentals=1_600_000, bytes_accessed=2_000_000),
     )(edge, sink_logit, query_rows, kv, vk)
 
@@ -160,114 +167,149 @@
     return lax.ppermute(value, "tp", ring(shift))
 
 
-def project_kernel(*refs):
-    pieces = (len(refs) - 1) // 2
-    out_ref = refs[-1]
-    total = dot(refs[0][...], refs[pieces][...])
-    for n in range(1, pieces):
-        total += dot(refs[n][...], refs[pieces + n][...])
+def project_kernel(own_ref, right_ref, left_ref, far_ref, weight_ref, fetched_ref, out_ref):
+    total = dot(own_ref[...], weight_ref[...])
+    for n, heads_ref in enumerate((right_ref, left_ref, far_ref)):
+        total += dot(heads_ref[...], fetched_ref[n])
     out_ref[...] = total.astype(BF16)
 
 
-def project(lefts, rights):
-    rows = lefts[0].shape[0]
-    width = rights[0].shape[1]
+def project(own, heads, weight, fetched):
+    rows = own.shape[0]
+    depth, width = weight.shape
     step = 512
+    left = pl.BlockSpec((rows, depth), lambda i: (0, 0))
     return pl.pallas_call(
         project_kernel,
         grid=(width // step,),
-        in_specs=[pl.BlockSpec(a.shape, lambda i: (0, 0)) for a in lefts]
-        + [pl.BlockSpec((b.shape[0], step), lambda i: (0, i)) for b in rights],
+        in_specs=[left] * 4
+        + [
+            pl.BlockSpec((depth, step), lambda i: (0, i)),
+            pl.BlockSpec((len(heads), depth, step), lambda i: (0, 0, i)),
+        ],
         out_specs=pl.BlockSpec((rows, step), lambda i: (0, i)),
         out_shape=jax.ShapeDtypeStruct((rows, width), BF16),
         name="project",
+        compiler_params=pltpu.CompilerParams(vmem_limit_bytes=20 * 1024 * 1024),
         cost_estimate=pl.CostEstimate(flops=1_100_000_000, transcendentals=0, bytes_accessed=6_000_000),
-    )(*lefts, *rights)
+    )(own, *heads, weight, fetched)
 
 
 def fetch_weight(out_weight):
     peers = lax.axis_size("ep")
-    half = out_weight.shape[0] // 2
-    core = lax.axis_index("ep") % 2
-    mine = lax.dynamic_slice_in_dim(out_weight, core * half, half, 0)
-    swap = [(i, i ^ 1) for i in range(peers)]
+    me = lax.axis_index("ep")
+    quarter = me % 4
+    rows = out_weight.shape[0] // 4
+    mine = lax.dynamic_slice_in_dim(out_weight, quarter * rows, rows, 0)
     fetched = []
     for shift in (1, 3, 2):
-        a = shift_tp(mine, shift)
-        fetched.append((a, lax.ppermute(a, "ep", swap)))
-    return fetched
+        fetched.append(shift_tp(mine, shift))
+    first = jnp.stack(fetched)
+    second = lax.ppermute(first, "ep", [(i, i ^ 2) for i in range(peers)])
+    third = lax.ppermute(first, "ep", [(i, i ^ 1) for i in range(peers)])
+    fourth = lax.ppermute(second, "ep", [(i, i ^ 1) for i in range(peers)])
+    return first, third, second, fourth
+
+
+def join_weight(pieces):
+    count, rows, width = pieces[0].shape
+    quarter = lax.axis_index("ep") % 4
+    whole = jnp.zeros((count, 4, rows, width), BF16)
+    for n, piece in enumerate(pieces):
+        whole = lax.dynamic_update_slice_in_dim(whole, piece[:, None], quarter ^ n, 1)
+    return whole.reshape(count, 4 * rows, width)
 
 
 def mix_tokens(attended, out_weight, fetched):
     peers = lax.axis_size("tp")
     me = lax.axis_index("tp")
-    core = lax.axis_index("ep") % 2
     tokens = attended.shape[0] // peers
-    half = out_weight.shape[0] // 2
 
     def block(shift):
         return lax.dynamic_slice_in_dim(attended, (me + shift) % peers * tokens, tokens, 0)
 
-    lefts, rights = [block(0)], [out_weight]
-    for shift, (a, b) in zip((1, 3, 2), fetched):
-        heads = shift_tp(block(shift), shift)
-        lefts.append(lax.dynamic_slice_in_dim(heads, core * half, half, 1))
-        lefts.append(lax.dynamic_slice_in_dim(heads, (1 - core) * half, half, 1))
-        rights += [a, b]
-    return project(lefts, rights)
-
-
-def expert_kernel(*refs, pieces):
+    heads = []
+    for shift in (1, 3, 2):
+        heads.append(shift_tp(block(shift), shift))
+    return project(block(0), heads, out_weight, join_weight(fetched))
+
+
+def unpack_into(out_ref, base, packed_ref):
+    count = packed_ref.shape[0]
+    columns = packed_ref.shape[1] // CAP
+    last = packed_ref[:, columns * MAIN :, :].astype(F32)
+    for j in range(columns):
+        lanes = slice(j * 128, (j + 1) * 128)
+        tile = packed_ref[:, j * MAIN : (j + 1) * MAIN, :].astype(F32)
+        out_ref[base : base + count * MAIN, lanes] = tile.reshape(count * MAIN, 128).astype(BF16)
+        out_ref[base + count * MAIN : base + count * CAP, lanes] = last[:, j, :].astype(BF16)
+
+
+def expert_kernel(*refs, pieces, step, columns):
     rows = refs[:pieces]
-    gate_ref, up_ref, down_ref = refs[pieces : pieces + 3]
+    gate_hbm, up_hbm, down_hbm = refs[pieces : pieces + 3]
     outs = refs[pieces + 3 : 2 * pieces + 3]
-    joined, total = refs[2 * pieces + 3 :]
-    step = pl.program_id(0)
-    count = rows[0].shape[0]
-
-    @pl.when(step == 0)
-    def _():
+    joined, hidden, gate, up, down, gate_sem, up_sem, down_sem = refs[2 * pieces + 3 :]
+    count = joined.shape[0] // pieces
+
+    def part(source, target, sems, k, size):
+        lanes = pl.ds(pl.multiple_of(k * size, size), size)
+        return pltpu.make_async_copy(source.at[:, lanes], target.at[k], sems.at[k])
+
+    for k in range(gate.shape[0]):
+        part(gate_hbm, gate, gate_sem, k, step).start()
+        part(up_hbm, up, up_sem, k, step).start()
+    for k in range(down.shape[0]):
+        part(down_hbm, down, down_sem, k, columns).start()
+    for n in range(pieces):
+        unpack_into(joined, n * count, rows[n])
+
+    def first(k, carry):
+        part(gate_hbm, gate, gate_sem, k, step).wait()
+        part(up_hbm, up, up_sem, k, step).wait()
+        x = joined[...]
+        g = dot(x, gate[k])
+        hidden[k] = (g / (1.0 + jnp.exp(-g)) * dot(x, up[k])).astype(BF16)
+        return carry
+
+    lax.fori_loop(0, gate.shape[0], first, 0)
+
+    def second(k, carry):
+        part(down_hbm, down, down_sem, k, columns).wait()
+        h = jnp.concatenate([hidden[n] for n in range(hidden.shape[0])], axis=1)
+        out = dot(h, down[k]).astype(BF16)
+        lanes = pl.ds(pl.multiple_of(k * columns, columns), columns)
         for n in range(pieces):
-            joined[n * count : (n + 1) * count, :] = rows[n][...]
-
-    x = joined[...]
-    gate = dot(x, gate_ref[...])
-    up = dot(x, up_ref[...])
-    hidden = (gate / (1.0 + jnp.exp(-gate)) * up).astype(BF16)
-    part = dot(hidden, down_ref[...])
-
-    @pl.when(step == 0)
-    def _():
-        total[...] = part
-
-    @pl.when(step > 0)
-    def _():
-        total[...] += part
-
-    @pl.when(step == pl.num_programs(0) - 1)
-    def _():
-        for n in range(pieces):
-            outs[n][...] = total[n * count : (n + 1) * count, :].astype(BF16)
+            outs[n][:, lanes] = out[n * count : (n + 1) * count]
+        return carry
+
+    lax.fori_loop(0, down.shape[0], second, 0)
 
 
 def expert(rows, gate_weight, up_weight, down_weight):
     pieces = len(rows)
-    count, width = rows[0].shape
-    units = gate_weight.shape[1]
-    step = 256
-    whole = pl.BlockSpec((count, width), lambda i: (0, 0))
-    columns = pl.BlockSpec((width, step), lambda i: (0, i))
-    return pl.pallas_call(
-        functools.partial(expert_kernel, pieces=pieces),
-        grid=(units // step,),
-        in_specs=[whole] * pieces + [columns, columns, pl.BlockSpec((step, width), lambda i: (i, 0))],
-        out_specs=[whole] * pieces,
+    width, units = gate_weight.shape
+    count = rows[0].shape[0] * CAP
+    step, columns = 256, 1024
+    vmem = pl.BlockSpec(memory_space=pltpu.VMEM)
+    hbm = pl.BlockSpec(memory_space=pl.ANY)
+    return pl.pallas_call(
+        functools.partial(expert_kernel, pieces=pieces, step=step, columns=columns),
+        in_specs=[vmem] * pieces + [hbm] * 3,
+        out_specs=[vmem] * pieces,
         out_shape=[jax.ShapeDtypeStruct((count, width), BF16)] * pieces,
         scratch_shapes=[
             pltpu.VMEM((pieces * count, width), BF16),
-            pltpu.VMEM((pieces * count, width), F32),
+            pltpu.VMEM((units // step, pieces * count, step), BF16),
+            pltpu.VMEM((units // step, width, step), BF16),
+            pltpu.VMEM((units // step, width, step), BF16),
+            pltpu.VMEM((width // columns, units, columns), BF16),
+            pltpu.SemaphoreType.DMA((units // step,)),
+            pltpu.SemaphoreType.DMA((units // step,)),
+            pltpu.SemaphoreType.DMA((width // columns,)),
         ],
         name="expert",
+        compiler_params=pltpu.CompilerParams(vmem_limit_bytes=36 * 1024 * 1024),
         cost_estimate=pl.CostEstimate(
             flops=6 * pieces * count * width * units,
             transcendentals=pieces * count * units,
@@ -276,22 +318,52 @@
     )(*rows, gate_weight, up_weight, down_weight)
 
 
-def unpack(packed):
-    count = packed.shape[0]
-    columns = packed.shape[1] // CAP
-    main = packed[:, : columns * MAIN].reshape(count, columns, MAIN, 128)
-    main = main.transpose(0, 2, 1, 3).reshape(count * MAIN, columns * 128)
-    last = packed[:, columns * MAIN :].reshape(count, columns * 128)
-    return jnp.concatenate([main, last], axis=0)
-
-
-def pack(rows):
-    count = rows.shape[0] // CAP
-    columns = rows.shape[1] // 128
-    main = rows[: count * MAIN].reshape(count, MAIN, columns, 128)
-    main = main.transpose(0, 2, 1, 3).reshape(count, columns * MAIN, 128)
-    last = rows[count * MAIN :].reshape(count, columns, 128)
-    return jnp.concatenate([main, last], axis=1)
+def combine_kernel(packed_ref, high_ref, low_ref, out_ref, rows):
+    unpack_into(rows, 0, packed_ref)
+    back = rows[...]
+    slots = ((0,), (0,))
+    out_ref[...] = (dot(high_ref[...], back, slots) + dot(low_ref[...], back, slots)).astype(BF16)
+
+
+def combine(packed, high, low):
+    slots, tokens = high.shape
+    width = packed.shape[1] // CAP * 128
+    return pl.pallas_call(
+        combine_kernel,
+        out_shape=jax.ShapeDtypeStruct((tokens, width), BF16),
+        scratch_shapes=[pltpu.VMEM((slots, width), BF16)],
+        name="combine",
+        compiler_params=pltpu.CompilerParams(vmem_limit_bytes=20 * 1024 * 1024),
+        cost_estimate=pl.CostEstimate(flops=300_000_000, transcendentals=0, bytes_accessed=2_000_000),
+    )(packed, high, low)
+
+
+def sum_kernel(*refs):
+    out_ref = refs[-1]
+    for half in range(2):
+        parts = refs[3 * half : 3 * half + 3]
+        rows = parts[0][...].astype(F32) + parts[1][...].astype(F32) + parts[2][...].astype(F32)
+        count = rows.shape[0] // CAP
+        columns = rows.shape[1] // 128
+        here = slice(half * count, (half + 1) * count)
+        last = []
+        for j in range(columns):
+            piece = rows[:, j * 128 : (j + 1) * 128]
+            tile = piece[: count * MAIN].reshape(count, MAIN, 128).astype(BF16)
+            out_ref[here, j * MAIN : (j + 1) * MAIN, :] = tile
+            last.append(piece[count * MAIN :])
+        out_ref[here, columns * MAIN :, :] = jnp.stack(last, axis=1).astype(BF16)
+
+
+def sum_rows(low, high):
+    count, width = low[0].shape
+    return pl.pallas_call(
+        sum_kernel,
+        out_shape=jax.ShapeDtypeStruct((2 * count // CAP, CAP * width // 128, 128), BF16),
+        name="sum_rows",
+        compiler_params=pltpu.CompilerParams(vmem_limit_bytes=20 * 1024 * 1024),
+        cost_estimate=pl.CostEstimate(flops=2_000_000, transcendentals=0, bytes_accessed=5_000_000),
+    )(*low, *high)
 
 
 def swap_experts(packed):
@@ -300,7 +372,7 @@
 
 def expert_rows(arrived, weights):
     half = arrived.shape[0] // 2
-    rows0, rows1 = unpack(arrived[:half]), unpack(arrived[half:])
+    rows0, rows1 = arrived[:half], arrived[half:]
     right0 = shift_tp(rows0, 1)
     left1 = shift_tp(rows1, 3)
     far0 = shift_tp(right0, 1)
@@ -317,9 +389,7 @@
     via1 = shift_tp(p_far1, 3)
     from1_0 = shift_tp((p_left0.astype(F32) + via0.astype(F32)).astype(BF16), 1)
     from3_1 = shift_tp((p_right1.astype(F32) + via1.astype(F32)).astype(BF16), 3)
-    low = own0.astype(F32) + from1_0.astype(F32) + from3_0.astype(F32)
-    high = own1.astype(F32) + from1_1.astype(F32) + from3_1.astype(F32)
-    return jnp.concatenate([pack(low.astype(BF16)), pack(high.astype(BF16))])
+    return sum_rows((own0, from1_0, from3_0), (own1, from1_1, from3_1)), p_right0, p_right1
 
 
 def body(
@@ -339,15 +409,17 @@
     experts = lax.axis_size("ep")
     fetched = fetch_weight(out_weight)
     sent = dispatch(routed_rows, norm_gain, routing, route_weight, experts)
-    attended = attention(query_rows, key_rows, value_rows, sink_logit)
-    mixed = mix_tokens(attended, out_weight, fetched)
+    halo = halo_rows(key_rows, value_rows)
     weights = (gate_weight[0], up_weight[0], down_weight[0])
     out, high, low = sent
     arrived = swap_experts(out)
-    summed = expert_rows(arrived, weights)
-    back = unpack(swap_experts(summed))
-    rows = ((0,), (0,))
-    return mixed, (dot(high, back, rows) + dot(low, back, rows)).astype(BF16)
+    summed, early, late = expert_rows(arrived, weights)
+    before, joined, after, _ = lax.optimization_barrier((*halo, early))
+    fetched, _ = lax.optimization_barrier((fetched, late))
+    attended = attention(query_rows, before, joined, after, sink_logit)
+    mixed = mix_tokens(attended, out_weight, fetched)
+    back = swap_experts(summed)
+    return mixed, combine(back, high, low)
 
 
 def solution(mesh):

time: 201 us -> 193 us (0.960)
  Pallas kernels: 76.4 us -> 54.1 us
  waiting for transfers between devices: 57.3 us -> 70.3 us
  local copies, waits for them, and re-layouts: 7.39 us -> 14.5 us
  other arithmetic: 7.44 us -> 0.88 us
    pallas_call x5 -> x7, Pallas kernels: 65.9 us -> 45.5 us  [the longest x4 38 us: expert(): pl.pallas_call(functools.partial(expert_kernel, pieces=pieces, step=step,...]
    ppermute x18, waiting for transfers between devices: 47.8 us -> 58.1 us  [shift_tp(): return lax.ppermute(value, 'tp', ring(shift))]
    unnamed x41 -> x36, local copies, waits for them, and re-layouts: 3.11 us -> 9.42 us
    dynamic_update_slice x0 -> x4, local copies, waits for them, and re-layouts: none -> 2.71 us  [join_weight(): lax.dynamic_update_slice_in_dim(whole, piece[:, None], quarter ^ n, 1)]
    all_to_all x2, waiting for transfers between devices: 9.59 us -> 12.2 us  [swap_experts(): return lax.all_to_all(packed, 'ep', 0, 0, tiled=True)]
    ppermute x5, starting transfers between devices: 4.28 us -> 6.61 us  [the longest x1 3.03 us: halo_rows(): before = lax.ppermute(joined[rows - WINDOW:], 'ep', up)]
  transfers between devices with their start and end apart: 25 -> 25, of which waited for: 8 -> 10; matrix products, arithmetic and copies ran while one was open for 6% -> 3% of each run, Pallas kernels for 37% -> 25%
where the time goes in v2:
time: 193 us; the launch traced here: 191 us
  waiting for transfers between devices  70.3 us (36%)
  Pallas kernels  54.1 us (28%)
  starting transfers between devices  50 us (26%)
  local copies, waits for them, and re-layouts  14.5 us (8%)
    ppermute x18, waiting for transfers between devices, shift_tp(): return lax.ppermute(value, 'tp', ring(shift))  58.1 us
    pallas_call x4, Pallas kernels, expert(): pl.pallas_call(functools.partial(expert_kernel, pieces=pieces, step=step,...  38 us
    ppermute x18, starting transfers between devices, shift_tp(): return lax.ppermute(value, 'tp', ring(shift))  28.2 us
    all_to_all x2, starting transfers between devices, swap_experts(): return lax.all_to_all(packed, 'ep', 0, 0, tiled=True)  15.2 us
    all_to_all x2, waiting for transfers between devices, swap_experts(): return lax.all_to_all(packed, 'ep', 0, 0, tiled=True)  12.2 us
    unnamed x36, local copies, waits for them, and re-layouts  9.42 us
    pallas_call x1, Pallas kernels, attention(): pl.pallas_call(attention_kernel, grid=(rows // WINDOW,), in_specs=[pl.Blo...  5.58 us
  transfers between devices with their start and end apart: 25, of which 10 were waited for; matrix products, arithmetic and copies ran while one was open for 3% of the time, Pallas kernels for 25%

profile of v2, /device:TPU:0, one launch (start us, length us, event | category | flops | bytes accessed | tf_op | source)
XLA Modules:
  0.0 190.9 jit_solution(13003947984052487907)
XLA Ops:
  0.7 3.0 %dispatch.1 = (bf16[32,144,128]{2,1,0:T(8,128)(2,1)}, bf16[288,128]{1,0:T(8,128)(2,1)}, bf16[288,128]{1,0:T(8,128)(2,1)}) custom-call(bf16[128,2048]{1,0:T(8,128)(2,1)} %rows_ref.1, f32[1,2048]{1,0:T(1,128)} %bitcast.44, s32[2,128]{1,0:T(2,128)} %bitcast.45, f32[2,128]{1,0:T(2,128)} %bitcast.46), custom_call_target="tpu_custom_call" | custom-call | flops 400000000 | bytes 2500000 | tf_op jit(solution)/shard_map/dispatch/pallas_call | solution.py:69
  3.6 8.4 %all-to-all-start = ((bf16[32,144,128]{2,1,0:T(8,128)(2,1)}), bf16[32,144,128]{2,1,0:T(8,128)(2,1)S(1)}, u32[]{:S(2)}, u32[]{:S(2)}) async-start(bf16[32,144,128]{2,1,0:T(8,128)(2,1)} %get-tuple-element.20), calls=%async_computation | async-start | bytes 2359296 | tf_op jit(solution)/shard_map/all_to_all | solution.py:370
  13.1 3.1 %collective-permute-start.9 = (bf16[64,2048]{1,0:T(8,128)(2,1)S(1)}, bf16[64,2048]{1,0:T(8,128)(2,1)S(1)}, u32[]{:S(2)}, u32[]{:S(2)}) collective-permute-start(bf16[64,2048]{1,0:T(8,128)(2,1)S(1)} %constant_dynamic-slice_fusion), channel_id=1, source_target_pairs={{0,2},{1,3},{2,0},{3,1},{4,6},{5,7},{6,4},{7,5},{8,10},{9,11},{10,... | collective-permute-start | bytes 786440 | tf_op jit(solution)/shard_map/ppermute | solution.py:167
  20.0 3.0 %collective-permute-start = (bf16[128,128]{1,0:T(8,128)(2,1)S(1)}, bf16[128,128]{1,0:T(8,128)(2,1)S(1)}, u32[]{:S(2)}, u32[]{:S(2)}) collective-permute-start(bf16[128,128]{1,0:T(8,128)(2,1)S(1)} %get-tuple-element.45), channel_id=1, source_target_pairs={{0,4},{4,8},{8,12},{12,16},{16,20},{20,24},{24,28},{28,32},{32,36}... | collective-permute-start | bytes 98312 | tf_op jit(solution)/shard_map/ppermute | solution.py:129
  23.9 5.0 %collective-permute-done.8 = bf16[64,2048]{1,0:T(8,128)(2,1)S(1)} collective-permute-done((bf16[64,2048]{1,0:T(8,128)(2,1)S(1)}, bf16[64,2048]{1,0:T(8,128)(2,1)S(1)}, u32[]{:S(2)}, u32[]{:S(2)}) %collective-permute-start.8) | collective-permute-done | bytes 262176 | tf_op jit(solution)/shard_map/ppermute | solution.py:167
  30.9 2.8 %collective-permute-start.3 = (bf16[16,144,128]{2,1,0:T(8,128)(2,1)S(1)}, bf16[16,144,128]{2,1,0:T(8,128)(2,1)S(1)}, u32[]{:S(2)}, u32[]{:S(2)}) collective-permute-start(bf16[16,144,128]{2,1,0:T(8,128)(2,1)S(1)} %get-tuple-element.38.refs_1_), channel_id=1, source_target_pairs={{0,3},{1,0},{2,1},{3,2},{4,7},{5,4},{6,5},{7,6},{8,11},{9,8},{10,9... | collective-permute-start | bytes 1769480 | tf_op jit(solution)/shard_map/ppermute | solution.py:167
  33.7 3.1 %copy-done.4 = bf16[1,2048,1792]{2,1,0:T(8,128)(2,1)S(1)} copy-done((bf16[1,2048,1792]{2,1,0:T(8,128)(2,1)S(1)}, bf16[1,2048,1792]{2,1,0:T(8,128)(2,1)}, u32[]{:S(2)}) %copy-start.4) | copy-done | bytes 7340056
  36.8 3.1 %copy-done.5 = bf16[1,2048,1792]{2,1,0:T(8,128)(2,1)S(1)} copy-done((bf16[1,2048,1792]{2,1,0:T(8,128)(2,1)S(1)}, bf16[1,2048,1792]{2,1,0:T(8,128)(2,1)}, u32[]{:S(2)}) %copy-start.5) | copy-done | bytes 7340056
  39.9 9.5 %expert.6 = (bf16[144,2048]{1,0:T(8,128)(2,1)S(1)}, bf16[144,2048]{1,0:T(8,128)(2,1)S(1)}) custom-call(bf16[16,144,128]{2,1,0:T(8,128)(2,1)S(1)} %get-tuple-element.39.refs_0_, bf16[16,144,128]{2,1,0:T(8,128)(2,1)S(1)} %get-tuple-element.38.refs_1_, bf16[2048,1792]{1,0:T(8,128)(2,1)S(1)} %bitcast.29, bf16[2048,1792]{1,0:T(8,128)(2,1)S(1)} %bitcast.33, ...), custom_call_target="tpu_custom_call" | custom-call | flops 6341787648 | bytes 22020096 | tf_op jit(solution)/shard_map/expert/pallas_call | solution.py:296
  50.8 9.5 %expert.4 = (bf16[144,2048]{1,0:T(8,128)(2,1)S(1)}, bf16[144,2048]{1,0:T(8,128)(2,1)S(1)}) custom-call(bf16[16,144,128]{2,1,0:T(8,128)(2,1)S(1)} %collective-permute-done.2.refs_0_, bf16[16,144,128]{2,1,0:T(8,128)(2,1)S(1)} %collective-permute-done.3.refs_1_, bf16[2048,1792]{1,0:T(8,128)(2,1)S(1)} %bitcast.30, bf16[2048,1792]{1,0:T(8,128)(2,1)S(1)} %bitcast.34, ...), custom_call_target="tpu_custom_call" | custom-call | flops 6341787648 | bytes 22020096 | tf_op jit(solution)/shard_map/expert/pallas_call | solution.py:296
  60.3 2.6 %collective-permute-start.14 = (bf16[16,144,128]{2,1,0:T(8,128)(2,1)S(1)}, bf16[16,144,128]{2,1,0:T(8,128)(2,1)S(1)}, u32[]{:S(2)}, u32[]{:S(2)}) collective-permute-start(bf16[16,144,128]{2,1,0:T(8,128)(2,1)S(1)} %get-tuple-element.39.refs_0_), channel_id=1, source_target_pairs={{0,3},{1,0},{2,1},{3,2},{4,7},{5,4},{6,5},{7,6},{8,11},{9,8},{10,9... | collective-permute-start | bytes 1769480 | tf_op jit(solution)/shard_map/ppermute | solution.py:167
  68.6 8.0 %collective-permute-done.14.refs_1_ = bf16[16,144,128]{2,1,0:T(8,128)(2,1)S(1)} collective-permute-done((bf16[16,144,128]{2,1,0:T(8,128)(2,1)S(1)}, bf16[16,144,128]{2,1,0:T(8,128)(2,1)S(1)}, u32[]{:S(2)}, u32[]{:S(2)}) %collective-permute-start.14) | collective-permute-done | bytes 589856 | tf_op jit(solution)/shard_map/ppermute | solution.py:167
  78.4 9.5 %expert.5 = (bf16[144,2048]{1,0:T(8,128)(2,1)S(1)}, bf16[144,2048]{1,0:T(8,128)(2,1)S(1)}) custom-call(bf16[16,144,128]{2,1,0:T(8,128)(2,1)S(1)} %collective-permute-done.13.refs_0_, bf16[16,144,128]{2,1,0:T(8,128)(2,1)S(1)} %collective-permute-done.14.refs_1_, bf16[2048,1792]{1,0:T(8,128)(2,1)S(1)} %bitcast.31, bf16[2048,1792]{1,0:T(8,128)(2,1)S(1)} %bitcast.35, ...), custom_call_target="tpu_custom_call" | custom-call | flops 6341787648 | bytes 22020096 | tf_op jit(solution)/shard_map/expert/pallas_call | solution.py:296
  88.0 13.0 %collective-permute-done.16.refs_1_ = bf16[16,144,128]{2,1,0:T(8,128)(2,1)S(1)} collective-permute-done((bf16[16,144,128]{2,1,0:T(8,128)(2,1)S(1)}, bf16[16,144,128]{2,1,0:T(8,128)(2,1)S(1)}, u32[]{:S(2)}, u32[]{:S(2)}) %collective-permute-start.16) | collective-permute-done | bytes 589856 | tf_op jit(solution)/shard_map/ppermute | solution.py:167
  101.0 9.5 %expert.7 = (bf16[144,2048]{1,0:T(8,128)(2,1)S(1)}, bf16[144,2048]{1,0:T(8,128)(2,1)S(1)}) custom-call(bf16[16,144,128]{2,1,0:T(8,128)(2,1)S(1)} %collective-permute-done.15.refs_0_, bf16[16,144,128]{2,1,0:T(8,128)(2,1)S(1)} %collective-permute-done.16.refs_1_, bf16[2048,1792]{1,0:T(8,128)(2,1)S(1)} %bitcast.32, bf16[2048,1792]{1,0:T(8,128)(2,1)S(1)} %bitcast.36, ...), custom_call_target="tpu_custom_call" | custom-call | flops 6341787648 | bytes 22020096 | tf_op jit(solution)/shard_map/expert/pallas_call | solution.py:296
  114.5 5.6 %attention.1 = bf16[1024,256]{1,0:T(8,128)(2,1)S(1)} custom-call(s32[2]{0:T(128)S(1)} %add_convert_fusion.2.edge_ref, f32[4]{0:T(128)S(1)} %copy-done.7, bf16[1024,256]{1,0:T(8,128)(2,1)S(1)} %copy-done.6, bf16[1280,128]{1,0:T(8,128)(2,1)S(1)} %constant_dynamic-update-slice_fusion.kv_ref, bf16[1280,128]{1,0:T(8,128)(2,1)S(1)} %pad_maximum_fusion.1.vk_ref), custom_call_target="tpu_custom_call" | custom-call | flops 4000000000 | bytes 2000000 | tf_op jit(solution)/shard_map/attention/pallas_call | solution.py:143
  120.1 6.9 %collective-permute-done.17 = bf16[144,2048]{1,0:T(8,128)(2,1)S(1)} collective-permute-done((bf16[144,2048]{1,0:T(8,128)(2,1)S(1)}, bf16[144,2048]{1,0:T(8,128)(2,1)S(1)}, u32[]{:S(2)}, u32[]{:S(2)}) %collective-permute-start.17) | collective-permute-done | bytes 589856 | tf_op jit(solution)/shard_map/ppermute | solution.py:167
  131.5 2.0 %collective-permute-start.6 = (bf16[256,256]{1,0:T(8,128)(2,1)}, bf16[256,256]{1,0:T(8,128)(2,1)S(1)}, u32[]{:S(2)}, u32[]{:S(2)}) collective-permute-start(bf16[256,256]{1,0:T(8,128)(2,1)} %get-tuple-element.40), channel_id=1, source_target_pairs={{0,2},{1,3},{2,0},{3,1},{4,6},{5,7},{6,4},{7,5},{8,10},{9,11},{10,... | collective-permute-start | bytes 393224 | tf_op jit(solution)/shard_map/ppermute | solution.py:167
  134.0 10.4 %collective-permute-done.20.refs_4_ = bf16[144,2048]{1,0:T(8,128)(2,1)S(1)} collective-permute-done((bf16[144,2048]{1,0:T(8,128)(2,1)S(1)}, bf16[144,2048]{1,0:T(8,128)(2,1)S(1)}, u32[]{:S(2)}, u32[]{:S(2)}) %collective-permute-start.20) | collective-permute-done | bytes 589856 | tf_op jit(solution)/shard_map/ppermute | solution.py:167
  146.4 12.5 %collective-permute-done.18.refs_1_ = bf16[144,2048]{1,0:T(8,128)(2,1)S(1)} collective-permute-done((bf16[144,2048]{1,0:T(8,128)(2,1)S(1)}, bf16[144,2048]{1,0:T(8,128)(2,1)S(1)}, u32[]{:S(2)}, u32[]{:S(2)}) %collective-permute-start.18) | collective-permute-done | bytes 589856 | tf_op jit(solution)/shard_map/ppermute | solution.py:167
  160.8 6.7 %all-to-all-start.1 = ((bf16[32,144,128]{2,1,0:T(8,128)(2,1)}), bf16[32,144,128]{2,1,0:T(8,128)(2,1)}, u32[]{:S(2)}, u32[]{:S(2)}) async-start(bf16[32,144,128]{2,1,0:T(8,128)(2,1)} %copy-done), calls=%async_computation.1 | async-start | bytes 2359296 | tf_op jit(solution)/shard_map/all_to_all | solution.py:370
  170.2 3.8 %project.1 = bf16[256,2048]{1,0:T(8,128)(2,1)} custom-call(bf16[256,256]{1,0:T(8,128)(2,1)S(1)} %get-tuple-element.43.own_ref, bf16[256,256]{1,0:T(8,128)(2,1)} %collective-permute-done.4.right_ref, bf16[256,256]{1,0:T(8,128)(2,1)S(1)} %collective-permute-done.5.left_ref, bf16[256,256]{1,0:T(8,128)(2,1)S(1)} %collective-permute-done.6.far_ref, ...), custom_call_target="tpu_custom_call" | custom-call | flops 1100000000 | bytes 6000000 | tf_op jit(solution)/shard_map/project/pallas_call | solution.py:182
  174.0 12.1 %all-to-all-done.1.packed_ref = bf16[32,144,128]{2,1,0:T(8,128)(2,1)} async-done(((bf16[32,144,128]{2,1,0:T(8,128)(2,1)}), bf16[32,144,128]{2,1,0:T(8,128)(2,1)}, u32[]{:S(2)}, u32[]{:S(2)}) %all-to-all-start.1) | async-done | bytes 1179680 | tf_op jit(solution)/shard_map/all_to_all | solution.py:370
  187.9 3.0 %combine.1 = bf16[128,2048]{1,0:T(8,128)(2,1)} custom-call(bf16[32,144,128]{2,1,0:T(8,128)(2,1)} %all-to-all-done.1.packed_ref, bf16[288,128]{1,0:T(8,128)(2,1)S(1)} %copy-done.2, bf16[288,128]{1,0:T(8,128)(2,1)S(1)} %copy-done.3), custom_call_target="tpu_custom_call" | custom-call | flops 300000000 | bytes 2000000 | tf_op jit(solution)/shard_map/combine/pallas_call | solution.py:331
  (88 shorter events, 33.6 us)
Async XLA Ops:
  3.6 27.1 %all-to-all-start = ((bf16[32,144,128]{2,1,0:T(8,128)(2,1)}), bf16[32,144,128]{2,1,0:T(8,128)(2,1)S(1)}, u32[]{:S(2)}, u32[]{:S(2)}) async-start(bf16[32,144,128]{2,1,0:T(8,128)(2,1)} %get-tuple-element.20), calls=%async_computation | async-start | bytes 2359296 | tf_op jit(solution)/shard_map/all_to_all | solution.py:370
  16.2 12.7 %collective-permute-start.8 = (bf16[64,2048]{1,0:T(8,128)(2,1)S(1)}, bf16[64,2048]{1,0:T(8,128)(2,1)S(1)}, u32[]{:S(2)}, u32[]{:S(2)}) collective-permute-start(bf16[64,2048]{1,0:T(8,128)(2,1)S(1)} %constant_dynamic-slice_fusion), channel_id=1, source_target_pairs={{0,3},{1,0},{2,1},{3,2},{4,7},{5,4},{6,5},{7,6},{8,11},{9,8},{10,9... | collective-permute-start | bytes 786440 | tf_op jit(solution)/shard_map/ppermute | solution.py:167
  17.3 11.6 %collective-permute-start.7 = (bf16[64,2048]{1,0:T(8,128)(2,1)S(1)}, bf16[64,2048]{1,0:T(8,128)(2,1)S(1)}, u32[]{:S(2)}, u32[]{:S(2)}) collective-permute-start(bf16[64,2048]{1,0:T(8,128)(2,1)S(1)} %constant_dynamic-slice_fusion), channel_id=1, source_target_pairs={{0,1},{1,2},{2,3},{3,0},{4,5},{5,6},{6,7},{7,4},{8,9},{9,10},{10,1... | collective-permute-start | bytes 786440 | tf_op jit(solution)/shard_map/ppermute | solution.py:167
  18.7 41.6 %collective-permute-start.1 = (bf16[128,128]{1,0:T(8,128)(2,1)S(1)}, bf16[128,128]{1,0:T(8,128)(2,1)S(1)}, u32[]{:S(2)}, u32[]{:S(2)}) collective-permute-start(bf16[128,128]{1,0:T(8,128)(2,1)S(1)} %get-tuple-element.44), channel_id=1, source_target_pairs={{4,0},{8,4},{12,8},{16,12},{20,16},{24,20},{28,24},{32,28},{36,32}... | collective-permute-start | bytes 98312 | tf_op jit(solution)/shard_map/ppermute | solution.py:130
  20.0 42.8 %collective-permute-start = (bf16[128,128]{1,0:T(8,128)(2,1)S(1)}, bf16[128,128]{1,0:T(8,128)(2,1)S(1)}, u32[]{:S(2)}, u32[]{:S(2)}) collective-permute-start(bf16[128,128]{1,0:T(8,128)(2,1)S(1)} %get-tuple-element.45), channel_id=1, source_target_pairs={{0,4},{4,8},{8,12},{12,16},{16,20},{20,24},{24,28},{28,32},{32,36}... | collective-permute-start | bytes 98312 | tf_op jit(solution)/shard_map/ppermute | solution.py:129
  29.0 20.4 %collective-permute-start.11 = (bf16[3,64,2048]{2,1,0:T(8,128)(2,1)S(1)}, bf16[3,64,2048]{2,1,0:T(8,128)(2,1)S(1)}, u32[]{:S(2)}, u32[]{:S(2)}) collective-permute-start(bf16[3,64,2048]{2,1,0:T(8,128)(2,1)S(1)} %pad_maximum_fusion), channel_id=1, source_target_pairs={{0,8},{4,12},{8,0},{12,4},{16,24},{20,28},{24,16},{28,20},{32,40},... | collective-permute-start | bytes 2359304 | tf_op jit(solution)/shard_map/ppermute | solution.py:208
  30.9 18.6 %collective-permute-start.3 = (bf16[16,144,128]{2,1,0:T(8,128)(2,1)S(1)}, bf16[16,144,128]{2,1,0:T(8,128)(2,1)S(1)}, u32[]{:S(2)}, u32[]{:S(2)}) collective-permute-start(bf16[16,144,128]{2,1,0:T(8,128)(2,1)S(1)} %get-tuple-element.38.refs_1_), channel_id=1, source_target_pairs={{0,3},{1,0},{2,1},{3,2},{4,7},{5,4},{6,5},{7,6},{8,11},{9,8},{10,9... | collective-permute-start | bytes 1769480 | tf_op jit(solution)/shard_map/ppermute | solution.py:167
  33.7 16.3 %collective-permute-start.2 = (bf16[16,144,128]{2,1,0:T(8,128)(2,1)S(1)}, bf16[16,144,128]{2,1,0:T(8,128)(2,1)S(1)}, u32[]{:S(2)}, u32[]{:S(2)}) collective-permute-start(bf16[16,144,128]{2,1,0:T(8,128)(2,1)S(1)} %get-tuple-element.39.refs_0_), channel_id=1, source_target_pairs={{0,1},{1,2},{2,3},{3,0},{4,5},{5,6},{6,7},{7,4},{8,9},{9,10},{10,1... | collective-permute-start | bytes 1769480 | tf_op jit(solution)/shard_map/ppermute | solution.py:167
  49.4 79.3 %collective-permute-start.10 = (bf16[3,64,2048]{2,1,0:T(8,128)(2,1)S(1)}, bf16[3,64,2048]{2,1,0:T(8,128)(2,1)S(1)}, u32[]{:S(2)}, u32[]{:S(2)}) collective-permute-start(bf16[3,64,2048]{2,1,0:T(8,128)(2,1)S(1)} %pad_maximum_fusion), channel_id=1, source_target_pairs={{0,4},{4,0},{8,12},{12,8},{16,20},{20,16},{24,28},{28,24},{32,36},... | collective-permute-start | bytes 2359304 | tf_op jit(solution)/shard_map/ppermute | solution.py:209
  49.5 81.9 %collective-permute-start.12 = (bf16[3,64,2048]{2,1,0:T(8,128)(2,1)S(1)}, bf16[3,64,2048]{2,1,0:T(8,128)(2,1)S(1)}, u32[]{:S(2)}, u32[]{:S(2)}) collective-permute-start(bf16[3,64,2048]{2,1,0:T(8,128)(2,1)S(1)} %collective-permute-done.11), channel_id=1, source_target_pairs={{0,4},{4,0},{8,12},{12,8},{16,20},{20,16},{24,28},{28,24},{32,36},... | collective-permute-start | bytes 2359304 | tf_op jit(solution)/shard_map/ppermute | solution.py:210
  50.0 16.8 %collective-permute-start.13 = (bf16[16,144,128]{2,1,0:T(8,128)(2,1)S(1)}, bf16[16,144,128]{2,1,0:T(8,128)(2,1)S(1)}, u32[]{:S(2)}, u32[]{:S(2)}) collective-permute-start(bf16[16,144,128]{2,1,0:T(8,128)(2,1)S(1)} %get-tuple-element.38.refs_1_), channel_id=1, source_target_pairs={{0,1},{1,2},{2,3},{3,0},{4,5},{5,6},{6,7},{7,4},{8,9},{9,10},{10,1... | collective-permute-start | bytes 1769480 | tf_op jit(solution)/shard_map/ppermute | solution.py:167
  60.3 16.3 %collective-permute-start.14 = (bf16[16,144,128]{2,1,0:T(8,128)(2,1)S(1)}, bf16[16,144,128]{2,1,0:T(8,128)(2,1)S(1)}, u32[]{:S(2)}, u32[]{:S(2)}) collective-permute-start(bf16[16,144,128]{2,1,0:T(8,128)(2,1)S(1)} %get-tuple-element.39.refs_0_), channel_id=1, source_target_pairs={{0,3},{1,0},{2,1},{3,2},{4,7},{5,4},{6,5},{7,6},{8,11},{9,8},{10,9... | collective-permute-start | bytes 1769480 | tf_op jit(solution)/shard_map/ppermute | solution.py:167
  62.8 82.1 %collective-permute-start.19 = (bf16[144,2048]{1,0:T(8,128)(2,1)S(1)}, bf16[144,2048]{1,0:T(8,128)(2,1)S(1)}, u32[]{:S(2)}, u32[]{:S(2)}) collective-permute-start(bf16[144,2048]{1,0:T(8,128)(2,1)S(1)} %get-tuple-element.21), channel_id=1, source_target_pairs={{0,3},{1,0},{2,1},{3,2},{4,7},{5,4},{6,5},{7,6},{8,11},{9,8},{10,9... | collective-permute-start | bytes 1769480 | tf_op jit(solution)/shard_map/ppermute | solution.py:167
  66.8 34.1 %collective-permute-start.16 = (bf16[16,144,128]{2,1,0:T(8,128)(2,1)S(1)}, bf16[16,144,128]{2,1,0:T(8,128)(2,1)S(1)}, u32[]{:S(2)}, u32[]{:S(2)}) collective-permute-start(bf16[16,144,128]{2,1,0:T(8,128)(2,1)S(1)} %collective-permute-done.3.refs_1_), channel_id=1, source_target_pairs={{0,3},{1,0},{2,1},{3,2},{4,7},{5,4},{6,5},{7,6},{8,11},{9,8},{10,9... | collective-permute-start | bytes 1769480 | tf_op jit(solution)/shard_map/ppermute | solution.py:167
  76.6 24.4 %collective-permute-start.15 = (bf16[16,144,128]{2,1,0:T(8,128)(2,1)S(1)}, bf16[16,144,128]{2,1,0:T(8,128)(2,1)S(1)}, u32[]{:S(2)}, u32[]{:S(2)}) collective-permute-start(bf16[16,144,128]{2,1,0:T(8,128)(2,1)S(1)} %collective-permute-done.2.refs_0_), channel_id=1, source_target_pairs={{0,1},{1,2},{2,3},{3,0},{4,5},{5,6},{6,7},{7,4},{8,9},{9,10},{10,1... | collective-permute-start | bytes 1769480 | tf_op jit(solution)/shard_map/ppermute | solution.py:167
  110.5 16.5 %collective-permute-start.17 = (bf16[144,2048]{1,0:T(8,128)(2,1)S(1)}, bf16[144,2048]{1,0:T(8,128)(2,1)S(1)}, u32[]{:S(2)}, u32[]{:S(2)}) collective-permute-start(bf16[144,2048]{1,0:T(8,128)(2,1)S(1)} %get-tuple-element.32), channel_id=1, source_target_pairs={{0,1},{1,2},{2,3},{3,0},{4,5},{5,6},{6,7},{7,4},{8,9},{9,10},{10,1... | collective-permute-start | bytes 1769480 | tf_op jit(solution)/shard_map/ppermute | solution.py:167
  112.6 14.5 %collective-permute-start.21 = (bf16[144,2048]{1,0:T(8,128)(2,1)S(1)}, bf16[144,2048]{1,0:T(8,128)(2,1)S(1)}, u32[]{:S(2)}, u32[]{:S(2)}) collective-permute-start(bf16[144,2048]{1,0:T(8,128)(2,1)S(1)} %get-tuple-element.35), channel_id=1, source_target_pairs={{0,3},{1,0},{2,1},{3,2},{4,7},{5,4},{6,5},{7,6},{8,11},{9,8},{10,9... | collective-permute-start | bytes 1769480 | tf_op jit(solution)/shard_map/ppermute | solution.py:167
  127.0 17.4 %collective-permute-start.20 = (bf16[144,2048]{1,0:T(8,128)(2,1)S(1)}, bf16[144,2048]{1,0:T(8,128)(2,1)S(1)}, u32[]{:S(2)}, u32[]{:S(2)}) collective-permute-start(bf16[144,2048]{1,0:T(8,128)(2,1)S(1)} %get-tuple-element.34), channel_id=1, source_target_pairs={{0,1},{1,2},{2,3},{3,0},{4,5},{5,6},{6,7},{7,4},{8,9},{9,10},{10,1... | collective-permute-start | bytes 1769480 | tf_op jit(solution)/shard_map/ppermute | solution.py:167
  127.1 31.8 %collective-permute-start.18 = (bf16[144,2048]{1,0:T(8,128)(2,1)S(1)}, bf16[144,2048]{1,0:T(8,128)(2,1)S(1)}, u32[]{:S(2)}, u32[]{:S(2)}) collective-permute-start(bf16[144,2048]{1,0:T(8,128)(2,1)S(1)} %add_convert_fusion.1), channel_id=1, source_target_pairs={{0,1},{1,2},{2,3},{3,0},{4,5},{5,6},{6,7},{7,4},{8,9},{9,10},{10,1... | collective-permute-start | bytes 1769480 | tf_op jit(solution)/shard_map/ppermute | solution.py:167
  128.8 30.2 %collective-permute-start.22 = (bf16[144,2048]{1,0:T(8,128)(2,1)S(1)}, bf16[144,2048]{1,0:T(8,128)(2,1)S(1)}, u32[]{:S(2)}, u32[]{:S(2)}) collective-permute-start(bf16[144,2048]{1,0:T(8,128)(2,1)S(1)} %add_convert_fusion), channel_id=1, source_target_pairs={{0,3},{1,0},{2,1},{3,2},{4,7},{5,4},{6,5},{7,6},{8,11},{9,8},{10,9... | collective-permute-start | bytes 1769480 | tf_op jit(solution)/shard_map/ppermute | solution.py:167
  131.5 38.7 %collective-permute-start.6 = (bf16[256,256]{1,0:T(8,128)(2,1)}, bf16[256,256]{1,0:T(8,128)(2,1)S(1)}, u32[]{:S(2)}, u32[]{:S(2)}) collective-permute-start(bf16[256,256]{1,0:T(8,128)(2,1)} %get-tuple-element.40), channel_id=1, source_target_pairs={{0,2},{1,3},{2,0},{3,1},{4,6},{5,7},{6,4},{7,5},{8,10},{9,11},{10,... | collective-permute-start | bytes 393224 | tf_op jit(solution)/shard_map/ppermute | solution.py:167
  144.4 25.8 %collective-permute-start.5 = (bf16[256,256]{1,0:T(8,128)(2,1)}, bf16[256,256]{1,0:T(8,128)(2,1)S(1)}, u32[]{:S(2)}, u32[]{:S(2)}) collective-permute-start(bf16[256,256]{1,0:T(8,128)(2,1)} %get-tuple-element.41), channel_id=1, source_target_pairs={{0,3},{1,0},{2,1},{3,2},{4,7},{5,4},{6,5},{7,6},{8,11},{9,8},{10,9... | collective-permute-start | bytes 393224 | tf_op jit(solution)/shard_map/ppermute | solution.py:167
  144.9 25.3 %collective-permute-start.4 = (bf16[256,256]{1,0:T(8,128)(2,1)}, bf16[256,256]{1,0:T(8,128)(2,1)}, u32[]{:S(2)}, u32[]{:S(2)}) collective-permute-start(bf16[256,256]{1,0:T(8,128)(2,1)} %get-tuple-element.42), channel_id=1, source_target_pairs={{0,1},{1,2},{2,3},{3,0},{4,5},{5,6},{6,7},{7,4},{8,9},{9,10},{10,1... | collective-permute-start | bytes 393224 | tf_op jit(solution)/shard_map/ppermute | solution.py:167
  160.8 25.4 %all-to-all-start.1 = ((bf16[32,144,128]{2,1,0:T(8,128)(2,1)}), bf16[32,144,128]{2,1,0:T(8,128)(2,1)}, u32[]{:S(2)}, u32[]{:S(2)}) async-start(bf16[32,144,128]{2,1,0:T(8,128)(2,1)} %copy-done), calls=%async_computation.1 | async-start | bytes 2359296 | tf_op jit(solution)/shard_map/all_to_all | solution.py:370
  (17 other events, 209.2 us)
